TPU v7x, 32 devices: a whole 2x2x4 slice. The times are simulated.
32 devices in a mesh: sp: 8 (over z, x), tp: 4 (over y, core).
Axes of the slice: x: 2, y: 2, z: 4, core: 2. Of those that a mesh axis runs over, the one named last changes fastest.
Arguments:
- tokens_in: bfloat16 [4096, 4096], P(('sp', 'tp')), may hold values from -64 to 64
- w_query: bfloat16 [4096, 2048], P(None, 'tp'), may hold values from -0.09375 to 0.09375
- w_key: bfloat16 [4096, 2048], P(None, 'tp'), may hold values from -0.09375 to 0.09375
- w_value: bfloat16 [4096, 2048], P(None, 'tp'), may hold values from -0.09375 to 0.09375
- w_out: bfloat16 [2048, 4096], P('tp'), may hold values from -1 to 1
Outputs:
- mixed: bfloat16 [4096, 4096], P(('sp', 'tp'))
- log_weight: float32 [32, 4096], P('tp', 'sp')
All inputs are finite; a program needn't handle non-finite values.
Results may differ from a plain program's by a relative error of at most 0.019.
Values may be sent and summed in bfloat16 or wider, within the bound.
No kernel may reach another device: no remote copies, remote signals or barrier semaphores. Data moves between devices by JAX's collectives and lax.ppermute only.
A program may use at most 128 MiB of HBM per device.

v0:
```python
import jax
import jax.numpy as jnp
from jax import lax
from jax.experimental import pallas as pl
from jax.experimental.pallas import tpu as pltpu
from jax.sharding import PartitionSpec as P

HEAD_DIM = 64
SIDE_SPAN = 64
MIDDLE_DILATION = 8
WIDEST_DILATION = 64


ROTARY_BASE = 500000.0
NEGATIVE = -1e30


def shifted(block, axis, distance):
    devices = range(lax.axis_size(axis))
    route = [(i - distance, i) for i in devices if i - distance in devices]
    return lax.ppermute(block, axis, route)


def rotate(block, positions):
    half_size = block.shape[-1] // 2
    freq = 1.0 / ROTARY_BASE ** (jnp.arange(half_size, dtype=jnp.float32) / half_size)
    angle = positions[:, None] * freq[None, :]
    cosine = jnp.cos(angle)[:, None, :]
    sine = jnp.sin(angle)[:, None, :]
    front = block[..., :half_size]
    back = block[..., half_size:]
    return jnp.concatenate([front * cosine - back * sine, back * cosine + front * sine], axis=-1)


def pattern_attend(query, keys, values, lead_rows, dilation_step, low_row, high_row):
    rows_total, head_count, head_size = query.shape
    class_len = rows_total // dilation_step
    first_class = lead_rows // dilation_step - SIDE_SPAN
    class_q = query.reshape(class_len, dilation_step, head_count, head_size)
    class_k = keys.reshape(keys.shape[0] // dilation_step, dilation_step, head_count, head_size)
    class_v = values.reshape(values.shape[0] // dilation_step, dilation_step, head_count, head_size)
    sub_k = class_k[first_class : first_class + class_len + 2 * SIDE_SPAN]
    sub_v = class_v[first_class : first_class + class_len + 2 * SIDE_SPAN]
    if class_len <= SIDE_SPAN:
        block_len = class_len
        block_count = 1
        win_k = sub_k[None]
        win_v = sub_v[None]
        blocks_q = class_q[None]
    else:
        block_len = SIDE_SPAN
        block_count = class_len // SIDE_SPAN
        part_k = sub_k.reshape(block_count + 2, SIDE_SPAN, dilation_step, head_count, head_size)
        part_v = sub_v.reshape(block_count + 2, SIDE_SPAN, dilation_step, head_count, head_size)
        win_k = jnp.concatenate([part_k[:-2], part_k[1:-1], part_k[2:]], axis=1)
        win_v = jnp.concatenate([part_v[:-2], part_v[1:-1], part_v[2:]], axis=1)
        blocks_q = class_q.reshape(block_count, SIDE_SPAN, dilation_step, head_count, head_size)
    width = block_len + 2 * SIDE_SPAN
    scores = jnp.einsum("nasht,nksht->nshak", blocks_q, win_k, preferred_element_type=jnp.float32)
    scores = scores * head_size ** (-0.5)
    q_index = jnp.arange(block_len, dtype=jnp.int32)
    k_index = jnp.arange(width, dtype=jnp.int32)
    b_index = jnp.arange(block_count, dtype=jnp.int32)
    s_index = jnp.arange(dilation_step, dtype=jnp.int32)
    in_band = jnp.abs(k_index[None, :] - SIDE_SPAN - q_index[:, None]) <= SIDE_SPAN
    key_position = (
        (first_class + b_index[:, None] * block_len + k_index[None, :]) * dilation_step
    )[:, None, :] + s_index[None, :, None]
    is_valid = (key_position >= low_row) & (key_position < high_row)
    keep_mask = in_band[None, None, None] & is_valid[:, :, None, None, :]
    scores = jnp.where(keep_mask, scores, NEGATIVE)
    maxima = jnp.max(scores, axis=-1, keepdims=True)
    expo = jnp.exp(scores - maxima)
    totals = jnp.sum(expo, axis=-1)
    numerator = jnp.einsum(
        "nshak,nksht->nasht", expo.astype(jnp.bfloat16), win_v, preferred_element_type=jnp.float32
    )
    totals_t = jnp.transpose(totals, (0, 3, 1, 2))
    result = (
        (numerator / totals_t[..., None])
        .astype(jnp.bfloat16)
        .reshape(rows_total, head_count, head_size)
    )
    log_sum = jnp.transpose(maxima[..., 0] + jnp.log(totals), (0, 3, 1, 2)).reshape(
        rows_total, head_count
    )
    return (result, log_sum)


def combine(results):
    sums = jnp.stack([item[1] for item in results], axis=0)
    peak = jnp.max(sums, axis=0)
    share = jnp.exp(sums - peak[None])
    weight_sum = share[0] + share[1] + share[2]
    accum = share[0][..., None] * results[0][0].astype(jnp.float32)
    accum = accum + share[1][..., None] * results[1][0].astype(jnp.float32)
    accum = accum + share[2][..., None] * results[2][0].astype(jnp.float32)
    attended = (accum / weight_sum[..., None]).astype(jnp.bfloat16)
    return (attended, peak + jnp.log(weight_sum))


def general_device(tokens_in, w_query, w_key, w_value, w_out):
    col_count = w_query.shape[1]
    head_count = col_count // HEAD_DIM
    piece = lax.all_gather(tokens_in, "tp", axis=0, tiled=True)
    projected = jnp.concatenate(
        [
            jnp.dot(piece, w_query, preferred_element_type=jnp.float32),
            jnp.dot(piece, w_key, preferred_element_type=jnp.float32),
            jnp.dot(piece, w_value, preferred_element_type=jnp.float32),
        ],
        axis=1,
    )
    rows_total = projected.shape[0]
    sp_size = lax.axis_size("sp")
    sp_place = lax.axis_index("sp")
    positions = (sp_place * rows_total + jnp.arange(rows_total, dtype=jnp.int32)).astype(
        jnp.float32
    )
    shape3 = (rows_total, head_count, HEAD_DIM)
    query = rotate(projected[:, :col_count].reshape(shape3), positions).astype(jnp.bfloat16)
    keys = rotate(projected[:, col_count : 2 * col_count].reshape(shape3), positions).astype(
        jnp.bfloat16
    )
    values = projected[:, 2 * col_count :].astype(jnp.bfloat16).reshape(shape3)
    per_device_span = -(-(SIDE_SPAN * MIDDLE_DILATION) // rows_total)
    earlier_k = []
    earlier_v = []
    before_k, before_v = shifted((keys, values), "sp", 1)
    after_k, after_v = shifted((keys, values), "sp", -1)
    earlier_k.insert(0, before_k)
    earlier_v.insert(0, before_v)
    later_k = [after_k]
    later_v = [after_v]
    key_buf = jnp.concatenate(earlier_k + [keys] + later_k, axis=0)
    value_buf = jnp.concatenate(earlier_v + [values] + later_v, axis=0)
    lead_rows = per_device_span * rows_total
    low_row = lead_rows - sp_place * rows_total
    key_buf, value_buf, lead_rows, low_row, high_row = (
        key_buf,
        value_buf,
        lead_rows,
        low_row,
        low_row + sp_size * rows_total,
    )
    results = [
        pattern_attend(query, key_buf, value_buf, lead_rows, dilation_step, low_row, high_row)
        for dilation_step in (1, MIDDLE_DILATION)
    ]
    class_stride = WIDEST_DILATION // sp_size
    border_extent = SIDE_SPAN * class_stride
    class_shape = (rows_total // sp_size, sp_size, head_count, HEAD_DIM)
    parts = (
        lax.all_to_all(query.reshape(class_shape), "sp", split_axis=1, concat_axis=0, tiled=True),
        lax.all_to_all(keys.reshape(class_shape), "sp", split_axis=1, concat_axis=0, tiled=True),
        lax.all_to_all(values.reshape(class_shape), "sp", split_axis=1, concat_axis=0, tiled=True),
    )
    item_heads = parts[0].shape[2]
    flat = [item.reshape(rows_total, item_heads, HEAD_DIM) for item in parts]
    pad_k = jnp.pad(flat[1], ((border_extent, border_extent), (0, 0), (0, 0)))
    pad_v = jnp.pad(flat[2], ((border_extent, border_extent), (0, 0), (0, 0)))
    result, log_sum = pattern_attend(
        flat[0],
        pad_k,
        pad_v,
        border_extent,
        class_stride,
        border_extent,
        border_extent + rows_total,
    )
    result_back = lax.all_to_all(
        result.reshape(rows_total, 1, item_heads, HEAD_DIM),
        "sp",
        split_axis=0,
        concat_axis=1,
        tiled=True,
    )
    sum_back = lax.all_to_all(
        log_sum.reshape(rows_total, 1, item_heads), "sp", split_axis=0, concat_axis=1, tiled=True
    )
    results.append((result_back.reshape(shape3), sum_back.reshape(rows_total, head_count)))
    attended, log_weight = combine(results)
    flat_out = attended.reshape(rows_total, col_count)
    mixed = lax.psum_scatter(
        jnp.dot(flat_out, w_out, preferred_element_type=jnp.float32).astype(jnp.bfloat16),
        "tp",
        scatter_dimension=0,
        tiled=True,
    )
    return (mixed, jnp.transpose(log_weight, (1, 0)))


LANES = 128


def sin_tables(positions, lanes):
    half_size = HEAD_DIM // 2
    lane = jnp.arange(lanes, dtype=jnp.int32)
    step = (lane % half_size).astype(jnp.float32)
    freq = 1.0 / ROTARY_BASE ** (step / half_size)
    angle = positions.astype(jnp.float32)[:, None] * freq[None, :]
    sign = jnp.where(lane % HEAD_DIM < half_size, -1.0, 1.0)
    return jnp.cos(angle), jnp.sin(angle) * sign[None, :]


def turned(block, cosine, sine):
    rows, width = block.shape
    half_size = HEAD_DIM // 2
    lane = lax.broadcasted_iota(jnp.int32, (rows, width), 1)
    ahead = pltpu.roll(block, width - half_size, 1)
    behind = pltpu.roll(block, half_size, 1)
    other = jnp.where(lane % HEAD_DIM < half_size, ahead, behind)
    reps = width // cosine.shape[1]
    cosine = jnp.concatenate([cosine] * reps, axis=1)
    sine = jnp.concatenate([sine] * reps, axis=1)
    return block * cosine + other * sine


def project_three(xs, wq_ref, wk_ref, wv_ref, cosine, sine):
    scale = HEAD_DIM ** (-0.5)
    q = jnp.dot(xs[...], wq_ref[...], preferred_element_type=jnp.float32)
    q = (turned(q, cosine, sine) * scale).astype(jnp.bfloat16)
    k = jnp.dot(xs[...], wk_ref[...], preferred_element_type=jnp.float32)
    k = turned(k, cosine, sine).astype(jnp.bfloat16)
    v = jnp.dot(xs[...], wv_ref[...], preferred_element_type=jnp.float32)
    return q, k, v.astype(jnp.bfloat16)


def fill_pair(place, mine_ref, peer_ref, xs):
    rows = mine_ref.shape[0]
    core = place[1]
    xs[pl.ds(pl.multiple_of(core * rows, rows), rows), :] = mine_ref[...]
    xs[pl.ds(pl.multiple_of((1 - core) * rows, rows), rows), :] = peer_ref[...]


def near_kernel(place, mine_ref, peer_ref, wq_ref, wk_ref, wv_ref, cos_ref, sin_ref, out_ref, xs):
    @pl.when(pl.program_id(0) == 0)
    def _():
        fill_pair(place, mine_ref, peer_ref, xs)

    parts = project_three(xs, wq_ref, wk_ref, wv_ref, cos_ref[...], sin_ref[...])
    for n in range(3):
        out_ref[n] = parts[n]


def far_kernel(
    place, mine_ref, peer_ref, wq_ref, wk_ref, wv_ref, cos_ref, sin_ref, near_ref,
    nat_ref, send_ref, head_ref, tail_ref, xs, perm,
):
    rows = nat_ref.shape[1]
    half = rows // 2
    classes, _, per_class, _ = send_ref.shape

    @pl.when(pl.program_id(0) == 0)
    def _():
        fill_pair(place, mine_ref, peer_ref, xs)
        target = lax.broadcasted_iota(jnp.int32, (rows, rows), 0)
        source = lax.broadcasted_iota(jnp.int32, (rows, rows), 1)
        wanted = (target % per_class) * classes + target // per_class
        perm[...] = jnp.where(source == wanted, 1.0, 0.0).astype(jnp.bfloat16)

    parts = project_three(xs, wq_ref, wk_ref, wv_ref, cos_ref[...], sin_ref[...])
    row = place[0]
    near_at = pl.multiple_of(row * half, half)
    far_at = pl.multiple_of((1 - row) * half, half)
    for n in range(3):
        nat_ref[n, pl.ds(near_at, half), :] = near_ref[n]
        nat_ref[n, pl.ds(far_at, half), :] = parts[n]
        whole = nat_ref[n]
        moved = jnp.dot(perm[...], whole, preferred_element_type=jnp.float32)
        moved = moved.astype(jnp.bfloat16)
        for c in range(classes):
            send_ref[c, n] = moved[c * per_class : (c + 1) * per_class]
        if n:
            head_ref[n - 1] = nat_ref[n, :SIDE_SPAN, :]
            tail_ref[n - 1] = nat_ref[n, rows - SIDE_SPAN :, :]


def soft_pair(q, k, v, bias):
    lane = lax.broadcasted_iota(jnp.int32, q.shape, 1)
    outs = []
    sums = []
    for h in range(LANES // HEAD_DIM):
        own = (lane // HEAD_DIM) == h
        q_h = jnp.where(own, q, jnp.zeros_like(q))
        s = lax.dot_general(
            q_h, k, (((1,), (1,)), ((), ())), preferred_element_type=jnp.float32
        )
        s = s + bias
        top = jnp.max(s, axis=1, keepdims=True)
        e = jnp.exp(s - top)
        total = jnp.sum(e, axis=1, keepdims=True)
        o = jnp.dot(e.astype(jnp.bfloat16), v, preferred_element_type=jnp.float32)
        outs.append(o / total)
        sums.append(top + jnp.log(total))
    rows = q.shape[0]
    lane = lax.broadcasted_iota(jnp.int32, (rows, LANES), 1)
    result = outs[0]
    for h in range(1, len(outs)):
        result = jnp.where(lane // HEAD_DIM == h, outs[h], result)
    return result, sums


def place_sums(sums, step, rows):
    lane = lax.broadcasted_iota(jnp.int32, (rows, LANES), 1)
    out = jnp.zeros((rows, LANES), jnp.float32)
    for h in range(len(sums)):
        out = jnp.where(lane == step * len(sums) + h, sums[h], out)
    return out


def local_kernel(edge, qkv_ref, before_ref, after_ref, out_ref, lse_ref, ks, vs):
    rows = qkv_ref.shape[1]
    step = pl.program_id(0)
    for n, buf in ((1, ks), (2, vs)):
        buf[:SIDE_SPAN] = before_ref[n - 1]
        buf[SIDE_SPAN : SIDE_SPAN + rows] = qkv_ref[n]
        buf[SIDE_SPAN + rows :] = after_ref[n - 1]
    block = 2 * SIDE_SPAN
    width = block + 2 * SIDE_SPAN
    r = lax.broadcasted_iota(jnp.int32, (block, width), 0)
    c = lax.broadcasted_iota(jnp.int32, (block, width), 1)
    band = jnp.where(jnp.abs(c - SIDE_SPAN - r) <= SIDE_SPAN, 0.0, NEGATIVE)
    first = jnp.where(c < SIDE_SPAN, edge[0].astype(jnp.float32) * NEGATIVE, 0.0)
    last = jnp.where(c >= width - SIDE_SPAN, edge[1].astype(jnp.float32) * NEGATIVE, 0.0)

    @pl.when(step == 0)
    def _():
        lse_ref[...] = jnp.zeros_like(lse_ref)

    count = rows // block
    for b in range(count):
        bias = band
        if b == 0:
            bias = bias + first
        if b == count - 1:
            bias = bias + last
        at = slice(b * block, (b + 1) * block)
        keys = slice(b * block, b * block + width)
        o, sums = soft_pair(qkv_ref[0, at, :], ks[keys], vs[keys], bias)
        out_ref[at, :] = o.astype(jnp.bfloat16)
        lse_ref[at, :] += place_sums(sums, step, block)


def wide_kernel(near_step, far_step, qkv_ref, out_ref, bias, lse):
    sources, _, per, lanes = qkv_ref.shape
    rows = sources * per
    step = pl.program_id(0)
    block = 128

    @pl.when(step == 0)
    def _():
        lse[...] = jnp.zeros_like(lse)
        for b in range(rows // block):
            r = lax.broadcasted_iota(jnp.int32, (block, rows), 0) + b * block
            c = lax.broadcasted_iota(jnp.int32, (block, rows), 1)
            gap = jnp.abs(r - c)
            near = (gap % near_step == 0) & (gap <= SIDE_SPAN * near_step)
            far = (gap % far_step == 0) & (gap <= SIDE_SPAN * far_step)
            one = jnp.where(near | far, 0.0, NEGATIVE)
            bias[b * block : (b + 1) * block] = jnp.where(near & far, jnp.log(2.0), one)

    q = qkv_ref[:, 0].reshape(rows, lanes)
    k = qkv_ref[:, 1].reshape(rows, lanes)
    v = qkv_ref[:, 2].reshape(rows, lanes)
    for b in range(rows // block):
        at = slice(b * block, (b + 1) * block)
        o, sums = soft_pair(q[at], k, v, bias[at])
        first = b * block // per
        o = o.astype(jnp.bfloat16).reshape(block // per, per, lanes)
        lane_at = pl.ds(pl.multiple_of(step * lanes, lanes), lanes)
        out_ref[first : first + block // per, :, lane_at] = o
        lse[at] += place_sums(sums, step, block)

    @pl.when(step == pl.num_programs(0) - 1)
    def _():
        heads = pl.num_programs(0) * (LANES // HEAD_DIM)
        value = lse[...]
        high = value.astype(jnp.bfloat16).astype(jnp.float32)
        middle = (value - high).astype(jnp.bfloat16).astype(jnp.float32)
        low = value - high - middle
        packed = high + pltpu.roll(middle, heads, 1) + pltpu.roll(low, 2 * heads, 1)
        packed = packed.astype(jnp.bfloat16).reshape(sources, per, LANES)
        out_ref[:, :, out_ref.shape[2] - LANES :] = packed


def merge_kernel(tp_place, near_ref, lse_ref, wide_ref, att_ref, lw_ref, flat):
    rows, cols = near_ref.shape
    sources, per, width = wide_ref.shape
    heads = lw_ref.shape[0]
    for c in range(sources):
        flat[c * per : (c + 1) * per] = wide_ref[c]
    block = rows // 4
    lane = lax.broadcasted_iota(jnp.int32, (block, LANES), 1)
    for b in range(rows // block):
        r = lax.broadcasted_iota(jnp.int32, (block, rows), 0) + b * block
        m = lax.broadcasted_iota(jnp.int32, (block, rows), 1)
        pick = jnp.where(m == (r % sources) * per + r // sources, 1.0, 0.0)
        wide = jnp.dot(pick.astype(jnp.bfloat16), flat[...], preferred_element_type=jnp.float32)
        at = slice(b * block, (b + 1) * block)
        parts = wide[:, width - LANES :]
        l_wide = parts + pltpu.roll(parts, LANES - heads, 1)
        l_wide = l_wide + pltpu.roll(parts, LANES - 2 * heads, 1)
        l_near = lse_ref[at, :]
        peak = jnp.maximum(l_near, l_wide)
        s_near = jnp.exp(l_near - peak)
        s_wide = jnp.exp(l_wide - peak)
        total = s_near + s_wide
        lw = peak + jnp.log(total)
        lw_ref[:, at] = jnp.transpose(lw)[:heads]
        w_near = s_near / total
        w_wide = s_wide / total
        slot = 3 - jnp.bitwise_xor(b, tp_place[0])
        to = pl.ds(pl.multiple_of(slot * block, block), block)
        for g in range(cols // LANES):
            h = 2 * g
            even = lane < HEAD_DIM
            a = jnp.where(even, w_near[:, h : h + 1], w_near[:, h + 1 : h + 2])
            z = jnp.where(even, w_wide[:, h : h + 1], w_wide[:, h + 1 : h + 2])
            cut = slice(g * LANES, (g + 1) * LANES)
            o = a * near_ref[at, cut].astype(jnp.float32) + z * wide[:, cut]
            att_ref[to, cut] = o.astype(jnp.bfloat16)


def params(kib=56000):
    return pltpu.CompilerParams(
        vmem_limit_bytes=kib * 1024, dimension_semantics=("arbitrary",)
    )


def cost(flops, size):
    return pl.CostEstimate(flops=int(flops), bytes_accessed=int(size), transcendentals=0)


SCALARS = pl.BlockSpec(memory_space=pltpu.SMEM)


def fast_device(tokens_in, w_query, w_key, w_value, w_out):
    own_rows, depth = tokens_in.shape
    cols = w_query.shape[1]
    heads = cols // HEAD_DIM
    tp_size = lax.axis_size("tp")
    sp_size = lax.axis_size("sp")
    tp_place = lax.axis_index("tp")
    sp_place = lax.axis_index("sp")
    rows = own_rows * tp_size
    half = rows // 2
    per = rows // sp_size
    cross = [(i, i ^ 2) for i in range(tp_size)]
    beside = [(i, i ^ 1) for i in range(tp_size)]
    far_mine = lax.ppermute(tokens_in, "tp", cross)
    near_peer = lax.ppermute(tokens_in, "tp", beside)
    far_peer = lax.ppermute(far_mine, "tp", beside)
    y_place = tp_place // 2
    place = jnp.stack([y_place, tp_place % 2]).astype(jnp.int32)
    span = jnp.arange(half, dtype=jnp.int32)
    base = sp_place * rows
    near_tables = sin_tables(base + y_place * half + span, LANES)
    far_tables = sin_tables(base + (1 - y_place) * half + span, LANES)
    wide_cols = min(256, cols)
    steps = cols // wide_cols
    x_spec = pl.BlockSpec((own_rows, depth), lambda j: (0, 0))
    w_spec = pl.BlockSpec((depth, wide_cols), lambda j: (0, j))
    t_spec = pl.BlockSpec((half, LANES), lambda j: (0, 0))
    near_spec = pl.BlockSpec((3, half, wide_cols), lambda j: (0, 0, j))
    edge_spec = pl.BlockSpec((2, SIDE_SPAN, wide_cols), lambda j: (0, 0, j))
    work = 2 * half * depth * 3 * cols
    moved = 3 * depth * cols * 2
    bf16 = jnp.bfloat16
    near = pl.pallas_call(
        near_kernel,
        grid=(steps,),
        in_specs=[SCALARS, x_spec, x_spec, w_spec, w_spec, w_spec, t_spec, t_spec],
        out_specs=near_spec,
        out_shape=jax.ShapeDtypeStruct((3, half, cols), bf16),
        scratch_shapes=[pltpu.VMEM((half, depth), bf16)],
        compiler_params=params(),
        cost_estimate=cost(work, moved),
        name="near_project",
    )(place, tokens_in, near_peer, w_query, w_key, w_value, *near_tables)
    nat, send, head, tail = pl.pallas_call(
        far_kernel,
        grid=(steps,),
        in_specs=[SCALARS, x_spec, x_spec, w_spec, w_spec, w_spec, t_spec, t_spec, near_spec],
        out_specs=[
            pl.BlockSpec((3, rows, wide_cols), lambda j: (0, 0, j)),
            pl.BlockSpec((sp_size, 3, per, wide_cols), lambda j: (0, 0, 0, j)),
            edge_spec,
            edge_spec,
        ],
        out_shape=[
            jax.ShapeDtypeStruct((3, rows, cols), bf16),
            jax.ShapeDtypeStruct((sp_size, 3, per, cols), bf16),
            jax.ShapeDtypeStruct((2, SIDE_SPAN, cols), bf16),
            jax.ShapeDtypeStruct((2, SIDE_SPAN, cols), bf16),
        ],
        scratch_shapes=[pltpu.VMEM((half, depth), bf16), pltpu.VMEM((rows, rows), bf16)],
        compiler_params=params(),
        cost_estimate=cost(work, moved),
        name="far_project",
    )(place, far_mine, far_peer, w_query, w_key, w_value, *far_tables, near)
    gathered = lax.all_to_all(send, "sp", split_axis=0, concat_axis=0, tiled=True)
    before = shifted(tail, "sp", 1)
    after = shifted(head, "sp", -1)
    edge = jnp.stack([sp_place == 0, sp_place == sp_size - 1]).astype(jnp.int32)
    groups = cols // LANES
    halo_spec = pl.BlockSpec((2, SIDE_SPAN, LANES), lambda j: (0, 0, j))
    o_near, l_near = pl.pallas_call(
        local_kernel,
        grid=(groups,),
        in_specs=[
            SCALARS,
            pl.BlockSpec((3, rows, LANES), lambda j: (0, 0, j)),
            halo_spec,
            halo_spec,
        ],
        out_specs=[
            pl.BlockSpec((rows, LANES), lambda j: (0, j)),
            pl.BlockSpec((rows, LANES), lambda j: (0, 0)),
        ],
        out_shape=[
            jax.ShapeDtypeStruct((rows, cols), bf16),
            jax.ShapeDtypeStruct((rows, LANES), jnp.float32),
        ],
        scratch_shapes=[pltpu.VMEM((rows + 2 * SIDE_SPAN, LANES), bf16)] * 2,
        compiler_params=params(),
        cost_estimate=cost(4e9, 4e6),
        name="local_attend",
    )(edge, nat, before, after)
    wide = pl.pallas_call(
        lambda *refs: wide_kernel(MIDDLE_DILATION // sp_size, WIDEST_DILATION // sp_size, *refs),
        grid=(groups,),
        in_specs=[pl.BlockSpec((sp_size, 3, per, LANES), lambda j: (0, 0, 0, j))],
        out_specs=pl.BlockSpec((sp_size, per, cols + LANES), lambda j: (0, 0, 0)),
        out_shape=jax.ShapeDtypeStruct((sp_size, per, cols + LANES), bf16),
        scratch_shapes=[
            pltpu.VMEM((rows, rows), jnp.float32),
            pltpu.VMEM((rows, LANES), jnp.float32),
        ],
        compiler_params=params(),
        cost_estimate=cost(8e9, 4e6),
        name="wide_attend",
    )(gathered)
    back = lax.all_to_all(wide, "sp", split_axis=0, concat_axis=0, tiled=True)
    whole = pl.BlockSpec(memory_space=pltpu.VMEM)
    attended, log_weight = pl.pallas_call(
        merge_kernel,
        in_specs=[SCALARS, whole, whole, whole],
        out_specs=[whole, whole],
        out_shape=[
            jax.ShapeDtypeStruct((rows, cols), bf16),
            jax.ShapeDtypeStruct((heads, rows), jnp.float32),
        ],
        scratch_shapes=[pltpu.VMEM((rows, cols + LANES), bf16)],
        compiler_params=pltpu.CompilerParams(vmem_limit_bytes=24 * 2**20),
        cost_estimate=cost(2e9, 4e6),
        name="merge",
    )(tp_place.astype(jnp.int32)[None], o_near, l_near, back)

    def product(lo, hi):
        block = attended[lo * own_rows : hi * own_rows]
        return jnp.dot(block, w_out, preferred_element_type=jnp.float32)

    first = lax.ppermute(product(0, 1).astype(bf16), "tp", beside)
    second = (product(1, 2) + first.astype(jnp.float32)).astype(bf16)
    crossed = lax.ppermute(second, "tp", cross)
    third = lax.ppermute(product(2, 3).astype(bf16), "tp", beside)
    total = product(3, 4) + third.astype(jnp.float32)
    mixed = (total + crossed.astype(jnp.float32)).astype(bf16)
    return (mixed, log_weight)


def per_device(tokens_in, w_query, w_key, w_value, w_out):
    sp_size = lax.axis_size("sp")
    tp_size = lax.axis_size("tp")
    rows = tokens_in.shape[0] * tp_size
    fits = (
        tp_size == 4
        and MIDDLE_DILATION % sp_size == 0
        and WIDEST_DILATION % sp_size == 0
        and tokens_in.shape[0] == 2 * SIDE_SPAN
        and (rows // sp_size) % 16 == 0
        and 128 % (rows // sp_size) == 0
        and w_query.shape[1] % 256 == 0
        and 3 * (w_query.shape[1] // HEAD_DIM) <= LANES
    )
    chosen = fast_device if fits else general_device
    return chosen(tokens_in, w_query, w_key, w_value, w_out)


def solution(mesh):
    in_specs = (P(("sp", "tp"), None), P(None, "tp"), P(None, "tp"), P(None, "tp"), P("tp", None))
    out_specs = (P(("sp", "tp"), None), P("tp", "sp"))
    return jax.shard_map(
        per_device, mesh=mesh, in_specs=in_specs, out_specs=out_specs, check_vma=False
    )
```

profile of v0, /device:TPU:14, one launch (start us, length us, event | category | flops | bytes accessed | tf_op | source)
XLA Modules:
  0.0 169.9 jit_solution(12167118299384357120)
XLA Ops:
  1.2 24.6 %collective-permute-done.mine_ref = bf16[128,4096]{1,0:T(8,128)(2,1)S(1)} collective-permute-done((bf16[128,4096]{1,0:T(8,128)(2,1)}, bf16[128,4096]{1,0:T(8,128)(2,1)S(1)}, u32[]{:S(2)}, u32[]{:S(2)}) %collective-permute-start) | collective-permute-done | bytes 1048608 | tf_op jit(solution)/shard_map/ppermute | solution.py:451
  26.5 1.8 %fusion.1 = (f32[256,128]{1,0:T(8,128)}, f32[256,128]{1,0:T(8,128)}, f32[256,128]{1,0:T(8,128)}, f32[256,128]{1,0:T(8,128)}) fusion(f32[256]{0:T(256)S(1)} %get-tuple-element.26, f32[128]{0:T(128)S(1)} %get-tuple-element.24, f32[128]{0:T(128)S(1)} %get-tuple-element.25, f32[256]{0:T(256)S(1)} %get-tuple-element.27), kind=kLoop, calls=%fused_computation.9 | loop fusion | flops 131072 | bytes 527360 | tf_op jit(solution)/shard_map/mul | solution.py:203
  28.3 1.0 copy-done.5
  29.3 8.9 %near_project.1.near_ref = bf16[3,256,512]{2,1,0:T(8,128)(2,1)} custom-call(s32[2]{0:T(128)} %pad_add_fusion.place, bf16[128,4096]{1,0:T(8,128)(2,1)} %mine_ref.1, bf16[128,4096]{1,0:T(8,128)(2,1)} %copy-done.5, bf16[4096,512]{1,0:T(8,128)(2,1)} %wq_ref.3, bf16[4096,512]{1,0:T(8,128)(2,1)} %wk_ref.3, bf16[4096,512]{1,0:T(8,128)(2,1)} %wv_ref.3, ...), custom_call_target="tpu_custom_call" | custom-call | flops 3221225472 | bytes 12582912 | tf_op jit(solution)/shard_map/near_project/pallas_call | solution.py:470
  38.2 1.0 copy-done.4
  39.2 10.7 %far_project.1 = (bf16[3,512,512]{2,1,0:T(8,128)(2,1)}, bf16[8,3,64,512]{3,2,1,0:T(8,128)(2,1)}, bf16[2,64,512]{2,1,0:T(8,128)(2,1)}, bf16[2,64,512]{2,1,0:T(8,128)(2,1)}) custom-call(s32[2]{0:T(128)} %pad_add_fusion.place, bf16[128,4096]{1,0:T(8,128)(2,1)} %copy-done.3, bf16[128,4096]{1,0:T(8,128)(2,1)} %copy-done.4, bf16[4096,512]{1,0:T(8,128)(2,1)} %wq_ref.3, ...), custom_call_target="tpu_custom_call" | custom-call | flops 3221225472 | bytes 12582912 | tf_op jit(solution)/shard_map/far_project/pallas_call | solution.py:481
  49.9 41.7 %all_to_all.10.refs_0_ = bf16[8,3,64,512]{3,2,1,0:T(8,128)(2,1)} all-to-all(bf16[8,3,64,512]{3,2,1,0:T(8,128)(2,1)} %get-tuple-element.15), channel_id=1, replica_groups=mesh['sp'=8,'tp'=4] {'sp'}, dimensions={0} | all-to-all | bytes 3145728 | tf_op jit(solution)/shard_map/all_to_all | solution.py:502
  91.6 11.7 %wide_attend.1 = bf16[8,64,640]{2,1,0:T(8,128)(2,1)} custom-call(bf16[8,3,64,512]{3,2,1,0:T(8,128)(2,1)} %all_to_all.10.refs_0_), custom_call_target="tpu_custom_call" | custom-call | flops 8000000000 | bytes 4000000 | tf_op jit(solution)/shard_map/wide_attend/pallas_call | solution.py:530
  103.3 5.8 %all-to-all-start.1 = ((bf16[8,64,640]{2,1,0:T(8,128)(2,1)}), bf16[8,64,640]{2,1,0:T(8,128)(2,1)S(1)}, u32[]{:S(2)}, u32[]{:S(2)}) async-start(bf16[8,64,640]{2,1,0:T(8,128)(2,1)} %wide_attend.1), calls=%async_computation.1 | async-start | bytes 1310720 | tf_op jit(solution)/shard_map/all_to_all | solution.py:544
  109.1 3.4 %collective-permute-start.3 = (bf16[2,64,512]{2,1,0:T(8,128)(2,1)S(1)}, bf16[2,64,512]{2,1,0:T(8,128)(2,1)S(1)}, u32[]{:S(2)}, u32[]{:S(2)}) collective-permute-start(bf16[2,64,512]{2,1,0:T(8,128)(2,1)S(1)} %copy-done.7), channel_id=1, source_target_pairs={{0,4},{4,8},{8,12},{12,16},{16,20},{20,24},{24,28},{1,5},{5,9},{9,... | collective-permute-start | bytes 393224 | tf_op jit(solution)/shard_map/ppermute | solution.py:21
  112.5 2.7 %collective-permute-start.4 = (bf16[2,64,512]{2,1,0:T(8,128)(2,1)S(1)}, bf16[2,64,512]{2,1,0:T(8,128)(2,1)S(1)}, u32[]{:S(2)}, u32[]{:S(2)}) collective-permute-start(bf16[2,64,512]{2,1,0:T(8,128)(2,1)S(1)} %copy-done.6), channel_id=1, source_target_pairs={{4,0},{8,4},{12,8},{16,12},{20,16},{24,20},{28,24},{5,1},{9,5},{13... | collective-permute-start | bytes 393224 | tf_op jit(solution)/shard_map/ppermute | solution.py:21
  115.8 10.3 %collective-permute-done.3.before_ref = bf16[2,64,512]{2,1,0:T(8,128)(2,1)S(1)} collective-permute-done((bf16[2,64,512]{2,1,0:T(8,128)(2,1)S(1)}, bf16[2,64,512]{2,1,0:T(8,128)(2,1)S(1)}, u32[]{:S(2)}, u32[]{:S(2)}) %collective-permute-start.3) | collective-permute-done | bytes 131104 | tf_op jit(solution)/shard_map/ppermute | solution.py:21
  126.0 1.9 %collective-permute-done.4.after_ref = bf16[2,64,512]{2,1,0:T(8,128)(2,1)S(1)} collective-permute-done((bf16[2,64,512]{2,1,0:T(8,128)(2,1)S(1)}, bf16[2,64,512]{2,1,0:T(8,128)(2,1)S(1)}, u32[]{:S(2)}, u32[]{:S(2)}) %collective-permute-start.4) | collective-permute-done | bytes 131104 | tf_op jit(solution)/shard_map/ppermute | solution.py:21
  128.6 5.7 %local_attend.1 = (bf16[512,512]{1,0:T(8,128)(2,1)}, f32[512,128]{1,0:T(8,128)}) custom-call(s32[2]{0:T(128)} %add_convert_fusion.2.edge, bf16[3,512,512]{2,1,0:T(8,128)(2,1)} %get-tuple-element.10.qkv_ref, bf16[2,64,512]{2,1,0:T(8,128)(2,1)} %copy-done.8, bf16[2,64,512]{2,1,0:T(8,128)(2,1)} %copy-done.9), custom_call_target="tpu_custom_call" | custom-call | flops 4000000000 | bytes 4000000 | tf_op jit(solution)/shard_map/local_attend/pallas_call | solution.py:508
  134.3 1.0 copy-done
  135.3 0.9 copy-done.1
  136.2 2.8 %merge.1 = (bf16[512,512]{1,0:T(8,128)(2,1)S(1)}, f32[8,512]{1,0:T(8,128)}) custom-call(s32[1]{0:T(128)} %bitcast.tp_place, bf16[512,512]{1,0:T(8,128)(2,1)S(1)} %copy-done, f32[512,128]{1,0:T(8,128)S(1)} %copy-done.1, bf16[8,64,640]{2,1,0:T(8,128)(2,1)S(1)} %all-to-all-done.1.wide_ref), custom_call_target="tpu_custom_call" | custom-call | flops 2000000000 | bytes 4000000 | tf_op jit(solution)/shard_map/merge/pallas_call | solution.py:546
  139.0 0.7 convolution_convert_fusion
  139.8 0.7 convolution_convert_fusion.1
  141.1 1.4 collective-permute-done.6
  142.5 0.7 add_convert_fusion.1
  143.8 0.7 fusion.8
  144.5 24.0 %collective-permute-done.7 = bf16[128,4096]{1,0:T(8,128)(2,1)S(1)} collective-permute-done((bf16[128,4096]{1,0:T(8,128)(2,1)S(1)}, bf16[128,4096]{1,0:T(8,128)(2,1)S(1)}, u32[]{:S(2)}, u32[]{:S(2)}) %collective-permute-start.7) | collective-permute-done | bytes 1048608 | tf_op jit(solution)/shard_map/ppermute | solution.py:566
  168.5 1.4 add_convert_fusion
  (30 shorter events, 3.7 us)
Async XLA Ops:
  0.6 25.2 %collective-permute-start = (bf16[128,4096]{1,0:T(8,128)(2,1)}, bf16[128,4096]{1,0:T(8,128)(2,1)S(1)}, u32[]{:S(2)}, u32[]{:S(2)}) collective-permute-start(bf16[128,4096]{1,0:T(8,128)(2,1)} %mine_ref.1), channel_id=1, source_target_pairs={{0,2},{1,3},{2,0},{3,1},{4,6},{5,7},{6,4},{7,5},{8,10},{9,11},{10,... | collective-permute-start | bytes 3145736 | tf_op jit(solution)/shard_map/ppermute | solution.py:451
  1.2 27.1 %collective-permute-start.2 = (bf16[128,4096]{1,0:T(8,128)(2,1)}, bf16[128,4096]{1,0:T(8,128)(2,1)S(1)}, u32[]{:S(2)}, u32[]{:S(2)}) collective-permute-start(bf16[128,4096]{1,0:T(8,128)(2,1)} %mine_ref.1), channel_id=1, source_target_pairs={{0,1},{1,0},{2,3},{3,2},{4,5},{5,4},{6,7},{7,6},{8,9},{9,8},{10,11... | collective-permute-start | bytes 3145736 | tf_op jit(solution)/shard_map/ppermute | solution.py:452
  25.8 12.4 %copy-start.3 = (bf16[128,4096]{1,0:T(8,128)(2,1)}, bf16[128,4096]{1,0:T(8,128)(2,1)S(1)}, u32[]{:S(2)}) copy-start(bf16[128,4096]{1,0:T(8,128)(2,1)S(1)} %collective-permute-done.mine_ref) | copy-start | bytes 3145732
  25.8 12.4 %collective-permute-start.1 = (bf16[128,4096]{1,0:T(8,128)(2,1)S(1)}, bf16[128,4096]{1,0:T(8,128)(2,1)S(1)}, u32[]{:S(2)}, u32[]{:S(2)}) collective-permute-start(bf16[128,4096]{1,0:T(8,128)(2,1)S(1)} %collective-permute-done.mine_ref), channel_id=1, source_target_pairs={{0,1},{1,0},{2,3},{3,2},{4,5},{5,4},{6,7},{7,6},{8,9},{9,8},{10,11... | collective-permute-start | bytes 3145736 | tf_op jit(solution)/shard_map/ppermute | solution.py:453
  28.3 1.0 copy-start.5
  38.2 1.0 copy-start.4
  91.6 17.5 %copy-start.7 = (bf16[2,64,512]{2,1,0:T(8,128)(2,1)S(1)}, bf16[2,64,512]{2,1,0:T(8,128)(2,1)}, u32[]{:S(2)}) copy-start(bf16[2,64,512]{2,1,0:T(8,128)(2,1)} %get-tuple-element.11) | copy-start | bytes 393220
  91.6 20.9 %copy-start.6 = (bf16[2,64,512]{2,1,0:T(8,128)(2,1)S(1)}, bf16[2,64,512]{2,1,0:T(8,128)(2,1)}, u32[]{:S(2)}) copy-start(bf16[2,64,512]{2,1,0:T(8,128)(2,1)} %get-tuple-element.12) | copy-start | bytes 393220
  103.3 30.9 %all-to-all-start.1 = ((bf16[8,64,640]{2,1,0:T(8,128)(2,1)}), bf16[8,64,640]{2,1,0:T(8,128)(2,1)S(1)}, u32[]{:S(2)}, u32[]{:S(2)}) async-start(bf16[8,64,640]{2,1,0:T(8,128)(2,1)} %wide_attend.1), calls=%async_computation.1 | async-start | bytes 1310720 | tf_op jit(solution)/shard_map/all_to_all | solution.py:544
  109.1 16.9 %collective-permute-start.3 = (bf16[2,64,512]{2,1,0:T(8,128)(2,1)S(1)}, bf16[2,64,512]{2,1,0:T(8,128)(2,1)S(1)}, u32[]{:S(2)}, u32[]{:S(2)}) collective-permute-start(bf16[2,64,512]{2,1,0:T(8,128)(2,1)S(1)} %copy-done.7), channel_id=1, source_target_pairs={{0,4},{4,8},{8,12},{12,16},{16,20},{20,24},{24,28},{1,5},{5,9},{9,... | collective-permute-start | bytes 393224 | tf_op jit(solution)/shard_map/ppermute | solution.py:21
  112.5 15.4 %collective-permute-start.4 = (bf16[2,64,512]{2,1,0:T(8,128)(2,1)S(1)}, bf16[2,64,512]{2,1,0:T(8,128)(2,1)S(1)}, u32[]{:S(2)}, u32[]{:S(2)}) collective-permute-start(bf16[2,64,512]{2,1,0:T(8,128)(2,1)S(1)} %copy-done.6), channel_id=1, source_target_pairs={{4,0},{8,4},{12,8},{16,12},{20,16},{24,20},{28,24},{5,1},{9,5},{13... | collective-permute-start | bytes 393224 | tf_op jit(solution)/shard_map/ppermute | solution.py:21
  126.0 1.9 %copy-start.8 = (bf16[2,64,512]{2,1,0:T(8,128)(2,1)}, bf16[2,64,512]{2,1,0:T(8,128)(2,1)S(1)}, u32[]{:S(2)}) copy-start(bf16[2,64,512]{2,1,0:T(8,128)(2,1)S(1)} %collective-permute-done.3.before_ref) | copy-start | bytes 393220
  127.9 0.7 copy-start.9
  134.2 1.0 copy-start
  135.3 0.9 copy-start.1
  136.2 2.8 %copy-start.2 = (bf16[512,4096]{1,0:T(8,128)(2,1)S(1)}, bf16[512,4096]{1,0:T(8,128)(2,1)}, u32[]{:S(2)}) copy-start(bf16[512,4096]{1,0:T(8,128)(2,1)} %param.9) | copy-start | bytes 12582916
  139.7 2.7 %collective-permute-start.6 = (bf16[128,4096]{1,0:T(8,128)(2,1)S(1)}, bf16[128,4096]{1,0:T(8,128)(2,1)S(1)}, u32[]{:S(2)}, u32[]{:S(2)}) collective-permute-start(bf16[128,4096]{1,0:T(8,128)(2,1)S(1)} %convolution_convert_fusion), channel_id=1, source_target_pairs={{0,1},{1,0},{2,3},{3,2},{4,5},{5,4},{6,7},{7,6},{8,9},{9,8},{10,11... | collective-permute-start | bytes 3145736 | tf_op jit(solution)/shard_map/ppermute | solution.py:564
  140.5 4.0 %collective-permute-start.5 = (bf16[128,4096]{1,0:T(8,128)(2,1)S(1)}, bf16[128,4096]{1,0:T(8,128)(2,1)S(1)}, u32[]{:S(2)}, u32[]{:S(2)}) collective-permute-start(bf16[128,4096]{1,0:T(8,128)(2,1)S(1)} %convolution_convert_fusion.1), channel_id=1, source_target_pairs={{0,1},{1,0},{2,3},{3,2},{4,5},{5,4},{6,7},{7,6},{8,9},{9,8},{10,11... | collective-permute-start | bytes 3145736 | tf_op jit(solution)/shard_map/ppermute | solution.py:567
  143.2 25.3 %collective-permute-start.7 = (bf16[128,4096]{1,0:T(8,128)(2,1)S(1)}, bf16[128,4096]{1,0:T(8,128)(2,1)S(1)}, u32[]{:S(2)}, u32[]{:S(2)}) collective-permute-start(bf16[128,4096]{1,0:T(8,128)(2,1)S(1)} %add_convert_fusion.1), channel_id=1, source_target_pairs={{0,2},{1,3},{2,0},{3,1},{4,6},{5,7},{6,4},{7,5},{8,10},{9,11},{10,... | collective-permute-start | bytes 3145736 | tf_op jit(solution)/shard_map/ppermute | solution.py:566
where the time goes:
time: 170 us
  waiting for transfers between devices  62.1 us (37%)
  blocking collectives  41.7 us (25%)
  Pallas kernels  39.7 us (23%)
  starting transfers between devices  13.6 us (8%)
  local copies, waits for them, and re-layouts  4.61 us (3%)
  other arithmetic  4.49 us (3%)
  matrix products  2.89 us (2%)
    all_to_all x1, blocking collectives, fast_device(): lax.all_to_all(send, 'sp', split_axis=0, concat_axis=0, tiled=True)  41.7 us
    ppermute x1, waiting for transfers between devices, fast_device(): far_mine = lax.ppermute(tokens_in, 'tp', cross)  24.6 us
    ppermute x1, waiting for transfers between devices, fast_device(): crossed = lax.ppermute(second, 'tp', cross)  24 us
    ppermute x2, waiting for transfers between devices, shifted(): return lax.ppermute(block, axis, route)  12.2 us
    pallas_call x1, Pallas kernels, fast_device(): pl.pallas_call(lambda *refs: wide_kernel(MIDDLE_DILATION // sp_size, WIDE...  11.7 us
    pallas_call x1, Pallas kernels, fast_device(): pl.pallas_call(far_kernel, grid=(steps,), in_specs=[SCALARS, x_spec, x_sp...  10.7 us
    pallas_call x1, Pallas kernels, fast_device(): pl.pallas_call(near_kernel, grid=(steps,), in_specs=[SCALARS, x_spec, x_s...  8.89 us
    ppermute x2, starting transfers between devices, shifted(): return lax.ppermute(block, axis, route)  6.01 us
  transfers between devices with their start and end apart: 9, of which 5 were waited for; matrix products, arithmetic and copies ran while one was open for 3% of the time, Pallas kernels for 9%

commit v1 on v0

--- a/solution.py
+++ b/solution.py
@@ -216,16 +216,6 @@
     return block * cosine + other * sine
 
 
-def project_three(xs, wq_ref, wk_ref, wv_ref, cosine, sine):
-    scale = HEAD_DIM ** (-0.5)
-    q = jnp.dot(xs[...], wq_ref[...], preferred_element_type=jnp.float32)
-    q = (turned(q, cosine, sine) * scale).astype(jnp.bfloat16)
-    k = jnp.dot(xs[...], wk_ref[...], preferred_element_type=jnp.float32)
-    k = turned(k, cosine, sine).astype(jnp.bfloat16)
-    v = jnp.dot(xs[...], wv_ref[...], preferred_element_type=jnp.float32)
-    return q, k, v.astype(jnp.bfloat16)
-
-
 def fill_pair(place, mine_ref, peer_ref, xs):
     rows = mine_ref.shape[0]
     core = place[1]
@@ -233,47 +223,41 @@
     xs[pl.ds(pl.multiple_of((1 - core) * rows, rows), rows), :] = peer_ref[...]
 
 
-def near_kernel(place, mine_ref, peer_ref, wq_ref, wk_ref, wv_ref, cos_ref, sin_ref, out_ref, xs):
-    @pl.when(pl.program_id(0) == 0)
-    def _():
-        fill_pair(place, mine_ref, peer_ref, xs)
-
-    parts = project_three(xs, wq_ref, wk_ref, wv_ref, cos_ref[...], sin_ref[...])
-    for n in range(3):
-        out_ref[n] = parts[n]
-
-
-def far_kernel(
-    place, mine_ref, peer_ref, wq_ref, wk_ref, wv_ref, cos_ref, sin_ref, near_ref,
-    nat_ref, send_ref, head_ref, tail_ref, xs, perm,
+def low_part(x, size):
+    return jnp.bitwise_and(x, size - 1)
+
+
+def high_part(x, size):
+    return jnp.right_shift(x, size.bit_length() - 1)
+
+
+def project_kernel(
+    place, mine_ref, peer_ref, wq_ref, wk_ref, wv_ref, cos_ref, sin_ref, qkv_ref, send_ref, xs,
 ):
-    rows = nat_ref.shape[1]
-    half = rows // 2
+    rows = qkv_ref.shape[1]
+    cols = qkv_ref.shape[2]
     classes, _, per_class, _ = send_ref.shape
-
-    @pl.when(pl.program_id(0) == 0)
-    def _():
-        fill_pair(place, mine_ref, peer_ref, xs)
-        target = lax.broadcasted_iota(jnp.int32, (rows, rows), 0)
-        source = lax.broadcasted_iota(jnp.int32, (rows, rows), 1)
-        wanted = (target % per_class) * classes + target // per_class
-        perm[...] = jnp.where(source == wanted, 1.0, 0.0).astype(jnp.bfloat16)
-
-    parts = project_three(xs, wq_ref, wk_ref, wv_ref, cos_ref[...], sin_ref[...])
-    row = place[0]
-    near_at = pl.multiple_of(row * half, half)
-    far_at = pl.multiple_of((1 - row) * half, half)
-    for n in range(3):
-        nat_ref[n, pl.ds(near_at, half), :] = near_ref[n]
-        nat_ref[n, pl.ds(far_at, half), :] = parts[n]
-        whole = nat_ref[n]
-        moved = jnp.dot(perm[...], whole, preferred_element_type=jnp.float32)
-        moved = moved.astype(jnp.bfloat16)
-        for c in range(classes):
-            send_ref[c, n] = moved[c * per_class : (c + 1) * per_class]
-        if n:
-            head_ref[n - 1] = nat_ref[n, :SIDE_SPAN, :]
-            tail_ref[n - 1] = nat_ref[n, rows - SIDE_SPAN :, :]
+    fill_pair(place, mine_ref, peer_ref, xs)
+    target = lax.broadcasted_iota(jnp.int32, (rows, rows), 0)
+    source = lax.broadcasted_iota(jnp.int32, (rows, rows), 1)
+    wanted = low_part(target, per_class) * classes + high_part(target, per_class)
+    perm = jnp.where(source == wanted, 1.0, 0.0).astype(jnp.bfloat16)
+    scale = HEAD_DIM ** (-0.5)
+    width = 256
+    for at in range(0, cols, width):
+        cut = slice(at, at + width)
+        for n, w_ref in enumerate((wq_ref, wk_ref, wv_ref)):
+            part = jnp.dot(xs[...], w_ref[:, cut], preferred_element_type=jnp.float32)
+            if n < 2:
+                part = turned(part, cos_ref[...], sin_ref[...])
+            if n == 0:
+                part = part * scale
+            part = part.astype(jnp.bfloat16)
+            qkv_ref[n, :, cut] = part
+            moved = jnp.dot(perm, part, preferred_element_type=jnp.float32)
+            moved = moved.astype(jnp.bfloat16)
+            for c in range(classes):
+                send_ref[c, n, :, cut] = moved[c * per_class : (c + 1) * per_class]
 
 
 def soft_pair(q, k, v, bias):
@@ -309,20 +293,26 @@
     return out
 
 
-def local_kernel(edge, qkv_ref, before_ref, after_ref, out_ref, lse_ref, ks, vs):
-    rows = qkv_ref.shape[1]
+def local_kernel(info, near_ref, far_ref, before_ref, after_ref, out_ref, lse_ref, qs, ks, vs):
+    half = near_ref.shape[1]
+    rows = 2 * half
     step = pl.program_id(0)
-    for n, buf in ((1, ks), (2, vs)):
-        buf[:SIDE_SPAN] = before_ref[n - 1]
-        buf[SIDE_SPAN : SIDE_SPAN + rows] = qkv_ref[n]
-        buf[SIDE_SPAN + rows :] = after_ref[n - 1]
+    y = info[2]
+    near_at = y * half
+    far_at = (1 - y) * half
+    for n, buf, lead in ((0, qs, 0), (1, ks, SIDE_SPAN), (2, vs, SIDE_SPAN)):
+        for at, ref in ((near_at, near_ref), (far_at, far_ref)):
+            buf[pl.ds(pl.multiple_of(at + lead, SIDE_SPAN), half), :] = ref[n]
+        if n:
+            buf[:SIDE_SPAN] = before_ref[n - 1]
+            buf[SIDE_SPAN + rows :] = after_ref[n - 1]
     block = 2 * SIDE_SPAN
     width = block + 2 * SIDE_SPAN
     r = lax.broadcasted_iota(jnp.int32, (block, width), 0)
     c = lax.broadcasted_iota(jnp.int32, (block, width), 1)
     band = jnp.where(jnp.abs(c - SIDE_SPAN - r) <= SIDE_SPAN, 0.0, NEGATIVE)
-    first = jnp.where(c < SIDE_SPAN, edge[0].astype(jnp.float32) * NEGATIVE, 0.0)
-    last = jnp.where(c >= width - SIDE_SPAN, edge[1].astype(jnp.float32) * NEGATIVE, 0.0)
+    first = jnp.where(c < SIDE_SPAN, info[0].astype(jnp.float32) * NEGATIVE, 0.0)
+    last = jnp.where(c >= width - SIDE_SPAN, info[1].astype(jnp.float32) * NEGATIVE, 0.0)
 
     @pl.when(step == 0)
     def _():
@@ -337,33 +327,45 @@
             bias = bias + last
         at = slice(b * block, (b + 1) * block)
         keys = slice(b * block, b * block + width)
-        o, sums = soft_pair(qkv_ref[0, at, :], ks[keys], vs[keys], bias)
-        out_ref[at, :] = o.astype(jnp.bfloat16)
-        lse_ref[at, :] += place_sums(sums, step, block)
-
-
-def wide_kernel(near_step, far_step, qkv_ref, out_ref, bias, lse):
-    sources, _, per, lanes = qkv_ref.shape
-    rows = sources * per
+        o, sums = soft_pair(qs[at], ks[keys], vs[keys], bias)
+        slot = jnp.bitwise_xor(y, b * block // half)
+        start = b * block % half
+        inner = slice(start, start + block)
+        out_ref[slot, inner, :] = o.astype(jnp.bfloat16)
+        lse_ref[slot, inner, :] += place_sums(sums, step, block)
+
+
+def wide_kernel(near_step, far_step, which, first_ref, second_ref, out_ref, bias, lse):
+    sources, _, per, lanes = first_ref.shape
+    half = sources * per
     step = pl.program_id(0)
     block = 128
+
+    def index_of(x, part):
+        return high_part(x, per) * (2 * per) + part * per + low_part(x, per)
 
     @pl.when(step == 0)
     def _():
         lse[...] = jnp.zeros_like(lse)
-        for b in range(rows // block):
-            r = lax.broadcasted_iota(jnp.int32, (block, rows), 0) + b * block
-            c = lax.broadcasted_iota(jnp.int32, (block, rows), 1)
-            gap = jnp.abs(r - c)
-            near = (gap % near_step == 0) & (gap <= SIDE_SPAN * near_step)
-            far = (gap % far_step == 0) & (gap <= SIDE_SPAN * far_step)
-            one = jnp.where(near | far, 0.0, NEGATIVE)
-            bias[b * block : (b + 1) * block] = jnp.where(near & far, jnp.log(2.0), one)
-
-    q = qkv_ref[:, 0].reshape(rows, lanes)
-    k = qkv_ref[:, 1].reshape(rows, lanes)
-    v = qkv_ref[:, 2].reshape(rows, lanes)
-    for b in range(rows // block):
+        for b in range(half // block):
+            r = lax.broadcasted_iota(jnp.int32, (block, half), 0) + b * block
+            r = index_of(r, which[0])
+            for k in range(2):
+                c = lax.broadcasted_iota(jnp.int32, (block, half), 1)
+                c = index_of(c, jnp.bitwise_xor(which[0], k))
+                gap = jnp.abs(r - c)
+                near = (low_part(gap, near_step) == 0) & (gap <= SIDE_SPAN * near_step)
+                far = (low_part(gap, far_step) == 0) & (gap <= SIDE_SPAN * far_step)
+                one = jnp.where(near | far, 0.0, NEGATIVE)
+                both = jnp.where(near & far, jnp.log(2.0), one)
+                bias[b * block : (b + 1) * block, k * half : (k + 1) * half] = both
+
+    q = first_ref[:, 0].reshape(half, lanes)
+    k = [ref[:, 1].reshape(half, lanes) for ref in (first_ref, second_ref)]
+    v = [ref[:, 2].reshape(half, lanes) for ref in (first_ref, second_ref)]
+    k = jnp.concatenate(k, axis=0)
+    v = jnp.concatenate(v, axis=0)
+    for b in range(half // block):
         at = slice(b * block, (b + 1) * block)
         o, sums = soft_pair(q[at], k, v, bias[at])
         first = b * block // per
@@ -384,24 +386,24 @@
         out_ref[:, :, out_ref.shape[2] - LANES :] = packed
 
 
-def merge_kernel(tp_place, near_ref, lse_ref, wide_ref, att_ref, lw_ref, flat):
-    rows, cols = near_ref.shape
+def merge_kernel(part, place, near_ref, lse_ref, wide_ref, att_ref, lw_ref, flat):
+    _, rows, cols = near_ref.shape
     sources, per, width = wide_ref.shape
     heads = lw_ref.shape[0]
     for c in range(sources):
         flat[c * per : (c + 1) * per] = wide_ref[c]
-    block = rows // 4
+    block = rows // 2
     lane = lax.broadcasted_iota(jnp.int32, (block, LANES), 1)
     for b in range(rows // block):
         r = lax.broadcasted_iota(jnp.int32, (block, rows), 0) + b * block
         m = lax.broadcasted_iota(jnp.int32, (block, rows), 1)
-        pick = jnp.where(m == (r % sources) * per + r // sources, 1.0, 0.0)
+        pick = jnp.where(m == low_part(r, sources) * per + high_part(r, sources), 1.0, 0.0)
         wide = jnp.dot(pick.astype(jnp.bfloat16), flat[...], preferred_element_type=jnp.float32)
         at = slice(b * block, (b + 1) * block)
         parts = wide[:, width - LANES :]
         l_wide = parts + pltpu.roll(parts, LANES - heads, 1)
         l_wide = l_wide + pltpu.roll(parts, LANES - 2 * heads, 1)
-        l_near = lse_ref[at, :]
+        l_near = lse_ref[part, at, :]
         peak = jnp.maximum(l_near, l_wide)
         s_near = jnp.exp(l_near - peak)
         s_wide = jnp.exp(l_wide - peak)
@@ -410,7 +412,7 @@
         lw_ref[:, at] = jnp.transpose(lw)[:heads]
         w_near = s_near / total
         w_wide = s_wide / total
-        slot = 3 - jnp.bitwise_xor(b, tp_place[0])
+        slot = 1 - jnp.bitwise_xor(b, place[1])
         to = pl.ds(pl.multiple_of(slot * block, block), block)
         for g in range(cols // LANES):
             h = 2 * g
@@ -418,7 +420,7 @@
             a = jnp.where(even, w_near[:, h : h + 1], w_near[:, h + 1 : h + 2])
             z = jnp.where(even, w_wide[:, h : h + 1], w_wide[:, h + 1 : h + 2])
             cut = slice(g * LANES, (g + 1) * LANES)
-            o = a * near_ref[at, cut].astype(jnp.float32) + z * wide[:, cut]
+            o = a * near_ref[part, at, cut].astype(jnp.float32) + z * wide[:, cut]
             att_ref[to, cut] = o.astype(jnp.bfloat16)
 
 
@@ -432,6 +434,7 @@
     return pl.CostEstimate(flops=int(flops), bytes_accessed=int(size), transcendentals=0)
 
 
+PROJECT_MIB = 40
 SCALARS = pl.BlockSpec(memory_space=pltpu.SMEM)
 
 
@@ -450,123 +453,124 @@
     beside = [(i, i ^ 1) for i in range(tp_size)]
     far_mine = lax.ppermute(tokens_in, "tp", cross)
     near_peer = lax.ppermute(tokens_in, "tp", beside)
-    far_peer = lax.ppermute(far_mine, "tp", beside)
     y_place = tp_place // 2
     place = jnp.stack([y_place, tp_place % 2]).astype(jnp.int32)
     span = jnp.arange(half, dtype=jnp.int32)
     base = sp_place * rows
     near_tables = sin_tables(base + y_place * half + span, LANES)
     far_tables = sin_tables(base + (1 - y_place) * half + span, LANES)
-    wide_cols = min(256, cols)
-    steps = cols // wide_cols
-    x_spec = pl.BlockSpec((own_rows, depth), lambda j: (0, 0))
-    w_spec = pl.BlockSpec((depth, wide_cols), lambda j: (0, j))
-    t_spec = pl.BlockSpec((half, LANES), lambda j: (0, 0))
-    near_spec = pl.BlockSpec((3, half, wide_cols), lambda j: (0, 0, j))
-    edge_spec = pl.BlockSpec((2, SIDE_SPAN, wide_cols), lambda j: (0, 0, j))
-    work = 2 * half * depth * 3 * cols
-    moved = 3 * depth * cols * 2
+    share = per // 2
     bf16 = jnp.bfloat16
-    near = pl.pallas_call(
-        near_kernel,
-        grid=(steps,),
-        in_specs=[SCALARS, x_spec, x_spec, w_spec, w_spec, w_spec, t_spec, t_spec],
-        out_specs=near_spec,
-        out_shape=jax.ShapeDtypeStruct((3, half, cols), bf16),
-        scratch_shapes=[pltpu.VMEM((half, depth), bf16)],
-        compiler_params=params(),
-        cost_estimate=cost(work, moved),
-        name="near_project",
-    )(place, tokens_in, near_peer, w_query, w_key, w_value, *near_tables)
-    nat, send, head, tail = pl.pallas_call(
-        far_kernel,
-        grid=(steps,),
-        in_specs=[SCALARS, x_spec, x_spec, w_spec, w_spec, w_spec, t_spec, t_spec, near_spec],
-        out_specs=[
-            pl.BlockSpec((3, rows, wide_cols), lambda j: (0, 0, j)),
-            pl.BlockSpec((sp_size, 3, per, wide_cols), lambda j: (0, 0, 0, j)),
-            edge_spec,
-            edge_spec,
-        ],
-        out_shape=[
-            jax.ShapeDtypeStruct((3, rows, cols), bf16),
-            jax.ShapeDtypeStruct((sp_size, 3, per, cols), bf16),
-            jax.ShapeDtypeStruct((2, SIDE_SPAN, cols), bf16),
-            jax.ShapeDtypeStruct((2, SIDE_SPAN, cols), bf16),
-        ],
-        scratch_shapes=[pltpu.VMEM((half, depth), bf16), pltpu.VMEM((rows, rows), bf16)],
-        compiler_params=params(),
-        cost_estimate=cost(work, moved),
-        name="far_project",
-    )(place, far_mine, far_peer, w_query, w_key, w_value, *far_tables, near)
-    gathered = lax.all_to_all(send, "sp", split_axis=0, concat_axis=0, tiled=True)
-    before = shifted(tail, "sp", 1)
-    after = shifted(head, "sp", -1)
-    edge = jnp.stack([sp_place == 0, sp_place == sp_size - 1]).astype(jnp.int32)
+    whole = pl.BlockSpec(memory_space=pltpu.VMEM)
+
+    def project(mine, peer, tables, name):
+        return pl.pallas_call(
+            project_kernel,
+            in_specs=[SCALARS] + [whole] * 7,
+            out_specs=[whole, whole],
+            out_shape=[
+                jax.ShapeDtypeStruct((3, half, cols), bf16),
+                jax.ShapeDtypeStruct((sp_size, 3, share, cols), bf16),
+            ],
+            scratch_shapes=[pltpu.VMEM((half, depth), bf16)],
+            compiler_params=pltpu.CompilerParams(vmem_limit_bytes=PROJECT_MIB * 2**20),
+            cost_estimate=cost(2 * half * depth * 3 * cols, 3 * depth * cols * 2),
+            name=name,
+        )(place, mine, peer, w_query, w_key, w_value, *tables)
+
+    def exchange(block):
+        shape = block.shape
+        flat = block.reshape(shape[0], -1, shape[-1])
+        flat = lax.all_to_all(flat, "sp", split_axis=0, concat_axis=0, tiled=True)
+        return flat.reshape(shape)
+
+    near, near_send = project(tokens_in, near_peer, near_tables, "near_project")
+    near_all = exchange(near_send)
+    near, far_mine = lax.optimization_barrier((near, far_mine))
+    far_peer = lax.ppermute(far_mine, "tp", beside)
+    far, far_send = project(far_mine, far_peer, far_tables, "far_project")
+    far_all = exchange(far_send)
+    low = jnp.where(y_place == 0, near[1:, :SIDE_SPAN], far[1:, :SIDE_SPAN])
+    top = jnp.where(y_place == 0, far[1:, half - SIDE_SPAN :], near[1:, half - SIDE_SPAN :])
+    before = shifted(top, "sp", 1)
+    after = shifted(low, "sp", -1)
+    info = jnp.stack([sp_place == 0, sp_place == sp_size - 1, y_place == 1]).astype(jnp.int32)
     groups = cols // LANES
     halo_spec = pl.BlockSpec((2, SIDE_SPAN, LANES), lambda j: (0, 0, j))
+    half_spec = pl.BlockSpec((3, half, LANES), lambda j: (0, 0, j))
     o_near, l_near = pl.pallas_call(
         local_kernel,
         grid=(groups,),
-        in_specs=[
-            SCALARS,
-            pl.BlockSpec((3, rows, LANES), lambda j: (0, 0, j)),
-            halo_spec,
-            halo_spec,
-        ],
+        in_specs=[SCALARS, half_spec, half_spec, halo_spec, halo_spec],
         out_specs=[
-            pl.BlockSpec((rows, LANES), lambda j: (0, j)),
-            pl.BlockSpec((rows, LANES), lambda j: (0, 0)),
+            pl.BlockSpec((2, half, LANES), lambda j: (0, 0, j)),
+            pl.BlockSpec((2, half, LANES), lambda j: (0, 0, 0)),
         ],
         out_shape=[
-            jax.ShapeDtypeStruct((rows, cols), bf16),
-            jax.ShapeDtypeStruct((rows, LANES), jnp.float32),
+            jax.ShapeDtypeStruct((2, half, cols), bf16),
+            jax.ShapeDtypeStruct((2, half, LANES), jnp.float32),
         ],
-        scratch_shapes=[pltpu.VMEM((rows + 2 * SIDE_SPAN, LANES), bf16)] * 2,
-        compiler_params=params(),
-        cost_estimate=cost(4e9, 4e6),
+        scratch_shapes=[pltpu.VMEM((rows, LANES), bf16)]
+        + [pltpu.VMEM((rows + 2 * SIDE_SPAN, LANES), bf16)] * 2,
+        compiler_params=params(16000),
+        cost_estimate=cost(6e9, 4e6),
         name="local_attend",
-    )(edge, nat, before, after)
-    wide = pl.pallas_call(
-        lambda *refs: wide_kernel(MIDDLE_DILATION // sp_size, WIDEST_DILATION // sp_size, *refs),
-        grid=(groups,),
-        in_specs=[pl.BlockSpec((sp_size, 3, per, LANES), lambda j: (0, 0, 0, j))],
-        out_specs=pl.BlockSpec((sp_size, per, cols + LANES), lambda j: (0, 0, 0)),
-        out_shape=jax.ShapeDtypeStruct((sp_size, per, cols + LANES), bf16),
-        scratch_shapes=[
-            pltpu.VMEM((rows, rows), jnp.float32),
-            pltpu.VMEM((rows, LANES), jnp.float32),
-        ],
-        compiler_params=params(),
-        cost_estimate=cost(8e9, 4e6),
-        name="wide_attend",
-    )(gathered)
-    back = lax.all_to_all(wide, "sp", split_axis=0, concat_axis=0, tiled=True)
-    whole = pl.BlockSpec(memory_space=pltpu.VMEM)
-    attended, log_weight = pl.pallas_call(
-        merge_kernel,
-        in_specs=[SCALARS, whole, whole, whole],
-        out_specs=[whole, whole],
-        out_shape=[
-            jax.ShapeDtypeStruct((rows, cols), bf16),
-            jax.ShapeDtypeStruct((heads, rows), jnp.float32),
-        ],
-        scratch_shapes=[pltpu.VMEM((rows, cols + LANES), bf16)],
-        compiler_params=pltpu.CompilerParams(vmem_limit_bytes=24 * 2**20),
-        cost_estimate=cost(2e9, 4e6),
-        name="merge",
-    )(tp_place.astype(jnp.int32)[None], o_near, l_near, back)
-
-    def product(lo, hi):
-        block = attended[lo * own_rows : hi * own_rows]
+    )(info, near, far, before, after)
+    all_spec = pl.BlockSpec((sp_size, 3, share, LANES), lambda j: (0, 0, 0, j))
+
+    def wide(which, first, second, name):
+        return pl.pallas_call(
+            lambda *refs: wide_kernel(MIDDLE_DILATION // sp_size, WIDEST_DILATION // sp_size, *refs),
+            grid=(groups,),
+            in_specs=[SCALARS, all_spec, all_spec],
+            out_specs=pl.BlockSpec((sp_size, share, cols + LANES), lambda j: (0, 0, 0)),
+            out_shape=jax.ShapeDtypeStruct((sp_size, share, cols + LANES), bf16),
+            scratch_shapes=[
+                pltpu.VMEM((half, rows), jnp.float32),
+                pltpu.VMEM((half, LANES), jnp.float32),
+            ],
+            compiler_params=params(16000),
+            cost_estimate=cost(6e9, 4e6),
+            name=name,
+        )(which.astype(jnp.int32)[None], first, second)
+
+    def merge(part, returned, name):
+        return pl.pallas_call(
+            lambda *refs: merge_kernel(part, *refs),
+            in_specs=[SCALARS, whole, whole, whole],
+            out_specs=[whole, whole],
+            out_shape=[
+                jax.ShapeDtypeStruct((half, cols), bf16),
+                jax.ShapeDtypeStruct((heads, half), jnp.float32),
+            ],
+            scratch_shapes=[pltpu.VMEM((half, cols + LANES), bf16)],
+            compiler_params=pltpu.CompilerParams(vmem_limit_bytes=16 * 2**20),
+            cost_estimate=cost(2e9, 4e6),
+            name=name,
+        )(place, o_near, l_near, returned)
+
+    far_wide = wide(1 - y_place, far_all, near_all, "far_wide")
+    far_back = exchange(far_wide)
+    near_first, near_second, _ = lax.optimization_barrier((near_all, far_all, far_wide))
+    near_wide = wide(y_place, near_first, near_second, "near_wide")
+    near_back = exchange(near_wide)
+    far_att, far_lw = merge(1, far_back, "far_merge")
+
+    def product(block):
         return jnp.dot(block, w_out, preferred_element_type=jnp.float32)
 
-    first = lax.ppermute(product(0, 1).astype(bf16), "tp", beside)
-    second = (product(1, 2) + first.astype(jnp.float32)).astype(bf16)
+    first = lax.ppermute(product(far_att[:own_rows]).astype(bf16), "tp", beside)
+    second = (product(far_att[own_rows:]) + first.astype(jnp.float32)).astype(bf16)
     crossed = lax.ppermute(second, "tp", cross)
-    third = lax.ppermute(product(2, 3).astype(bf16), "tp", beside)
-    total = product(3, 4) + third.astype(jnp.float32)
+    near_back, second = lax.optimization_barrier((near_back, second))
+    near_att, near_lw = merge(0, near_back, "near_merge")
+    third = lax.ppermute(product(near_att[:own_rows]).astype(bf16), "tp", beside)
+    total = product(near_att[own_rows:]) + third.astype(jnp.float32)
     mixed = (total + crossed.astype(jnp.float32)).astype(bf16)
+    swap = y_place == 0
+    log_weight = jnp.concatenate(
+        [jnp.where(swap, near_lw, far_lw), jnp.where(swap, far_lw, near_lw)], axis=1
+    )
     return (mixed, log_weight)
 
 
@@ -579,7 +583,7 @@
         and MIDDLE_DILATION % sp_size == 0
         and WIDEST_DILATION % sp_size == 0
         and tokens_in.shape[0] == 2 * SIDE_SPAN
-        and (rows // sp_size) % 16 == 0
+        and (rows // sp_size) % 32 == 0
         and 128 % (rows // sp_size) == 0
         and w_query.shape[1] % 256 == 0
         and 3 * (w_query.shape[1] // HEAD_DIM) <= LANES

time: 170 us -> 143 us (0.84); the launches traced: 170 us -> 141 us
  blocking collectives: 41.7 us -> 0 us
  waiting for transfers between devices: 62.1 us -> 34.4 us
  starting transfers between devices: 13.6 us -> 33.1 us
  local copies, waits for them, and re-layouts: 4.61 us -> 16.1 us
  matrix products: 2.89 us -> 7.52 us
  Pallas kernels: 39.7 us -> 43.8 us
    all_to_all x1 -> x0, blocking collectives: 41.7 us -> none  [fast_device(): lax.all_to_all(send, 'sp', split_axis=0, concat_axis=0, tiled=True)]
    ppermute x1, waiting for transfers between devices: 24.6 us -> 0.01 us  [fast_device(): far_mine = lax.ppermute(tokens_in, 'tp', cross)]
    all_to_all x1 -> x4, starting transfers between devices: 5.79 us -> 25.9 us  [exchange(): flat = lax.all_to_all(flat, 'sp', split_axis=0, concat_axis=0, tiled=True)]
    all_to_all x1 -> x4, waiting for transfers between devices: 0.01 us -> 14.1 us  [exchange(): flat = lax.all_to_all(flat, 'sp', split_axis=0, concat_axis=0, tiled=True)]
    ppermute x2, waiting for transfers between devices: 12.2 us -> 0.01 us  [shifted(): return lax.ppermute(block, axis, route)]
    unnamed x20 -> x26, local copies, waits for them, and re-layouts: 4.61 us -> 16.1 us
    ppermute x1, waiting for transfers between devices: 24 us -> 16.5 us  [fast_device(): crossed = lax.ppermute(second, 'tp', cross)]
    dot_general x4, matrix products: 2.89 us -> 7.52 us  [product(): return jnp.dot(block, w_out, preferred_element_type=jnp.float32)]
  transfers between devices with their start and end apart: 9 -> 12, of which waited for: 5 -> 5; matrix products, arithmetic and copies ran while one was open for 3% -> 6% of each run, Pallas kernels for 9% -> 30%
where the time goes in v1:
time: 143 us; the launch traced here: 141 us
  Pallas kernels  43.8 us (31%)
  waiting for transfers between devices  34.4 us (24%)
  starting transfers between devices  33.1 us (23%)
  local copies, waits for them, and re-layouts  16.1 us (11%)
  matrix products  7.52 us (5%)
  other arithmetic  5.3 us (4%)
    all_to_all x4, starting transfers between devices, exchange(): flat = lax.all_to_all(flat, 'sp', split_axis=0, concat_axis=0, tiled=True)  25.9 us
    pallas_call x2, Pallas kernels, project(): pl.pallas_call(project_kernel, in_specs=[SCALARS] + [whole] * 7, out_spec...  23 us
    ppermute x1, waiting for transfers between devices, fast_device(): crossed = lax.ppermute(second, 'tp', cross)  16.5 us
    unnamed x26, local copies, waits for them, and re-layouts  16.1 us
    all_to_all x4, waiting for transfers between devices, exchange(): flat = lax.all_to_all(flat, 'sp', split_axis=0, concat_axis=0, tiled=True)  14.1 us
    pallas_call x2, Pallas kernels, wide(): pl.pallas_call(lambda *refs: wide_kernel(MIDDLE_DILATION // sp_size, WIDE...  12.4 us
    dot_general x4, matrix products, product(): return jnp.dot(block, w_out, preferred_element_type=jnp.float32)  7.52 us
    ppermute x2, starting transfers between devices, shifted(): return lax.ppermute(block, axis, route)  6.02 us
  transfers between devices with their start and end apart: 12, of which 5 were waited for; matrix products, arithmetic and copies ran while one was open for 6% of the time, Pallas kernels for 30%

profile of v1, /device:TPU:14, one launch (start us, length us, event | category | flops | bytes accessed | tf_op | source)
XLA Modules:
  0.0 141.0 jit_solution(7286384454585747528)
XLA Ops:
  3.6 2.2 %copy-done = bf16[4096,512]{1,0:T(8,128)(2,1)S(1)} copy-done((bf16[4096,512]{1,0:T(8,128)(2,1)S(1)}, bf16[4096,512]{1,0:T(8,128)(2,1)}, u32[]{:S(2)}) %copy-start) | copy-done | bytes 4194328
  5.8 2.2 %copy-done.2 = bf16[4096,512]{1,0:T(8,128)(2,1)S(1)} copy-done((bf16[4096,512]{1,0:T(8,128)(2,1)S(1)}, bf16[4096,512]{1,0:T(8,128)(2,1)}, u32[]{:S(2)}) %copy-start.2) | copy-done | bytes 4194328
  9.2 11.5 %near_project.1 = (bf16[3,256,512]{2,1,0:T(8,128)(2,1)S(1)}, bf16[8,3,32,512]{3,2,1,0:T(8,128)(2,1)}) custom-call(s32[2]{0:T(128)S(1)} %pad_add_fusion.place.refs_0_, bf16[128,4096]{1,0:T(8,128)(2,1)S(1)} %copy-done.4, bf16[128,4096]{1,0:T(8,128)(2,1)S(1)} %collective-permute-done.peer_ref, bf16[4096,512]{1,0:T(8,128)(2,1)S(1)} %copy-done, ...), custom_call_target="tpu_custom_call" | custom-call | flops 3221225472 | bytes 12582912 | tf_op jit(solution)/shard_map/near_project/pallas_call | solution.py:467
  20.7 6.2 %all-to-all-start = ((bf16[8,96,512]{2,1,0:T(8,128)(2,1)}), bf16[8,96,512]{2,1,0:T(8,128)(2,1)S(1)}, u32[]{:S(2)}, u32[]{:S(2)}) async-start(bf16[8,96,512]{2,1,0:T(8,128)(2,1)} %bitcast.5), calls=%async_computation | async-start | bytes 1572864 | tf_op jit(solution)/shard_map/all_to_all | solution.py:484
  26.9 2.7 %collective-permute-done.2.peer_ref = bf16[128,4096]{1,0:T(8,128)(2,1)S(1)} collective-permute-done((bf16[128,4096]{1,0:T(8,128)(2,1)S(1)}, bf16[128,4096]{1,0:T(8,128)(2,1)S(1)}, u32[]{:S(2)}, u32[]{:S(2)}) %collective-permute-start.2) | collective-permute-done | bytes 1048608 | tf_op jit(solution)/shard_map/ppermute | solution.py:490
  29.6 2.2 %copy-done.1 = bf16[4096,512]{1,0:T(8,128)(2,1)S(1)} copy-done((bf16[4096,512]{1,0:T(8,128)(2,1)S(1)}, bf16[4096,512]{1,0:T(8,128)(2,1)}, u32[]{:S(2)}) %copy-start.1) | copy-done | bytes 4194328
  31.7 2.2 %copy-done.3 = bf16[4096,512]{1,0:T(8,128)(2,1)S(1)} copy-done((bf16[4096,512]{1,0:T(8,128)(2,1)S(1)}, bf16[4096,512]{1,0:T(8,128)(2,1)}, u32[]{:S(2)}) %copy-start.3) | copy-done | bytes 4194328
  33.9 11.5 %far_project.1 = (bf16[3,256,512]{2,1,0:T(8,128)(2,1)S(1)}, bf16[8,3,32,512]{3,2,1,0:T(8,128)(2,1)}) custom-call(s32[2]{0:T(128)S(1)} %pad_add_fusion.place.refs_0_, bf16[128,4096]{1,0:T(8,128)(2,1)S(1)} %collective-permute-done.1.mine_ref, bf16[128,4096]{1,0:T(8,128)(2,1)S(1)} %collective-permute-done.2.peer_ref, bf16[4096,512]{1,0:T(8,128)(2,1)S(1)} %copy-done.1, ...), custom_call_target="tpu_custom_call" | custom-call | flops 3221225472 | bytes 12582912 | tf_op jit(solution)/shard_map/far_project/pallas_call | solution.py:467
  46.4 6.0 %all-to-all-start.1 = ((bf16[8,96,512]{2,1,0:T(8,128)(2,1)}), bf16[8,96,512]{2,1,0:T(8,128)(2,1)S(1)}, u32[]{:S(2)}, u32[]{:S(2)}) async-start(bf16[8,96,512]{2,1,0:T(8,128)(2,1)} %bitcast.7), calls=%async_computation.1 | async-start | bytes 1572864 | tf_op jit(solution)/shard_map/all_to_all | solution.py:484
  53.4 3.4 %collective-permute-start.3 = (bf16[2,64,512]{2,1,0:T(8,128)(2,1)S(1)}, bf16[2,64,512]{2,1,0:T(8,128)(2,1)S(1)}, u32[]{:S(2)}, u32[]{:S(2)}) collective-permute-start(bf16[2,64,512]{2,1,0:T(8,128)(2,1)S(1)} %get-tuple-element.33), channel_id=1, source_target_pairs={{0,4},{4,8},{8,12},{12,16},{16,20},{20,24},{24,28},{1,5},{5,9},{9,... | collective-permute-start | bytes 393224 | tf_op jit(solution)/shard_map/ppermute | solution.py:21
  56.8 2.7 %collective-permute-start.4 = (bf16[2,64,512]{2,1,0:T(8,128)(2,1)S(1)}, bf16[2,64,512]{2,1,0:T(8,128)(2,1)S(1)}, u32[]{:S(2)}, u32[]{:S(2)}) collective-permute-start(bf16[2,64,512]{2,1,0:T(8,128)(2,1)S(1)} %get-tuple-element.32), channel_id=1, source_target_pairs={{4,0},{8,4},{12,8},{16,12},{20,16},{24,20},{28,24},{5,1},{9,5},{13... | collective-permute-start | bytes 393224 | tf_op jit(solution)/shard_map/ppermute | solution.py:21
  59.4 10.2 %all-to-all-done.1 = bf16[8,96,512]{2,1,0:T(8,128)(2,1)S(1)} async-done(((bf16[8,96,512]{2,1,0:T(8,128)(2,1)}), bf16[8,96,512]{2,1,0:T(8,128)(2,1)S(1)}, u32[]{:S(2)}, u32[]{:S(2)}) %all-to-all-start.1) | async-done | bytes 786464 | tf_op jit(solution)/shard_map/all_to_all | solution.py:484
  69.6 6.2 %far_wide.1 = bf16[8,32,640]{2,1,0:T(8,128)(2,1)} custom-call(s32[1]{0:T(128)} %bitcast.9.refs_0_, bf16[8,3,32,512]{3,2,1,0:T(8,128)(2,1)S(1)} %bitcast.16, bf16[8,3,32,512]{3,2,1,0:T(8,128)(2,1)S(1)} %bitcast.14), custom_call_target="tpu_custom_call" | custom-call | flops 6000000000 | bytes 4000000 | tf_op jit(solution)/shard_map/far_wide/pallas_call | solution.py:522
  75.8 7.6 %all-to-all-start.3 = ((bf16[8,32,640]{2,1,0:T(8,128)(2,1)}), bf16[8,32,640]{2,1,0:T(8,128)(2,1)S(1)}, u32[]{:S(2)}, u32[]{:S(2)}) async-start(bf16[8,32,640]{2,1,0:T(8,128)(2,1)} %far_wide.1), calls=%async_computation.3 | async-start | bytes 655360 | tf_op jit(solution)/shard_map/all_to_all | solution.py:484
  84.7 4.6 %local_attend.1 = (bf16[2,256,512]{2,1,0:T(8,128)(2,1)S(1)}, f32[2,256,128]{2,1,0:T(8,128)S(1)}) custom-call(s32[3]{0:T(128)S(1)} %add_convert_fusion.2.info, bf16[3,256,512]{2,1,0:T(8,128)(2,1)S(1)} %get-tuple-element.18.near_ref, bf16[3,256,512]{2,1,0:T(8,128)(2,1)S(1)} %copy-done.6, bf16[2,64,512]{2,1,0:T(8,128)(2,1)S(1)} %collective-permute-done.3.before_ref, ...), custom_call_target="tpu_custom_call" | custom-call | flops 6000000000 | bytes 4000000 | tf_op jit(solution)/shard_map/local_attend/pallas_call | solution.py:501
  92.8 1.9 %far_merge.1 = (bf16[256,512]{1,0:T(8,128)(2,1)S(1)}, f32[8,256]{1,0:T(8,128)S(1)}) custom-call(s32[2]{0:T(128)S(1)} %pad_add_fusion.place.refs_0_, bf16[2,256,512]{2,1,0:T(8,128)(2,1)S(1)} %copy-done.8, f32[2,256,128]{2,1,0:T(8,128)S(1)} %copy-done.10, bf16[8,32,640]{2,1,0:T(8,128)(2,1)S(1)} %all-to-all-done.3.refs_3_), custom_call_target="tpu_custom_call" | custom-call | flops 2000000000 | bytes 4000000 | tf_op jit(solution)/shard_map/far_merge/pallas_call | solution.py:538
  95.0 1.7 %convolution_convert_fusion.1 = bf16[128,4096]{1,0:T(8,128)(2,1)} fusion(bf16[512,4096]{1,0:T(8,128)(2,1)S(1)} %copy-done.11, bf16[256,512]{1,0:T(8,128)(2,1)S(1)} %get-tuple-element.27), kind=kOutput, calls=%fused_computation.1 | convolution fusion | flops 537395200 | bytes 5373952 | tf_op jit(solution)/shard_map/dot_general | solution.py:560
  96.7 6.2 %near_wide.1 = bf16[8,32,640]{2,1,0:T(8,128)(2,1)} custom-call(s32[1]{0:T(128)} %bitcast.refs_0_, bf16[8,3,32,512]{3,2,1,0:T(8,128)(2,1)S(1)} %bitcast.15, bf16[8,3,32,512]{3,2,1,0:T(8,128)(2,1)S(1)} %bitcast.17), custom_call_target="tpu_custom_call" | custom-call | flops 6000000000 | bytes 4000000 | tf_op jit(solution)/shard_map/near_wide/pallas_call | solution.py:522
  102.9 6.0 %all-to-all-start.2 = ((bf16[8,32,640]{2,1,0:T(8,128)(2,1)}), bf16[8,32,640]{2,1,0:T(8,128)(2,1)S(1)}, u32[]{:S(2)}, u32[]{:S(2)}) async-start(bf16[8,32,640]{2,1,0:T(8,128)(2,1)} %near_wide.1), calls=%async_computation.2 | async-start | bytes 655360 | tf_op jit(solution)/shard_map/all_to_all | solution.py:484
  108.9 4.2 %add_convert_fusion.1 = bf16[128,4096]{1,0:T(8,128)(2,1)} fusion(bf16[128,4096]{1,0:T(8,128)(2,1)} %collective-permute-done.5, bf16[512,4096]{1,0:T(8,128)(2,1)} %param.9, bf16[256,512]{1,0:T(8,128)(2,1)S(1)} %get-tuple-element.27), kind=kOutput, calls=%fused_computation.3 | convolution fusion | flops 538443776 | bytes 6422528 | tf_op jit(solution)/shard_map/dot_general | solution.py:560
  113.7 3.9 %all-to-all-done.2.refs_3_ = bf16[8,32,640]{2,1,0:T(8,128)(2,1)S(1)} async-done(((bf16[8,32,640]{2,1,0:T(8,128)(2,1)}), bf16[8,32,640]{2,1,0:T(8,128)(2,1)S(1)}, u32[]{:S(2)}, u32[]{:S(2)}) %all-to-all-start.2) | async-done | bytes 327712 | tf_op jit(solution)/shard_map/all_to_all | solution.py:484
  117.6 1.9 %near_merge.1 = (bf16[256,512]{1,0:T(8,128)(2,1)S(1)}, f32[8,256]{1,0:T(8,128)S(1)}) custom-call(s32[2]{0:T(128)S(1)} %pad_add_fusion.place.refs_0_, bf16[2,256,512]{2,1,0:T(8,128)(2,1)S(1)} %copy-done.8, f32[2,256,128]{2,1,0:T(8,128)S(1)} %copy-done.10, bf16[8,32,640]{2,1,0:T(8,128)(2,1)S(1)} %all-to-all-done.2.refs_3_), custom_call_target="tpu_custom_call" | custom-call | flops 2000000000 | bytes 4000000 | tf_op jit(solution)/shard_map/near_merge/pallas_call | solution.py:538
  122.0 16.5 %collective-permute-done.7 = bf16[128,4096]{1,0:T(8,128)(2,1)} collective-permute-done((bf16[128,4096]{1,0:T(8,128)(2,1)}, bf16[128,4096]{1,0:T(8,128)(2,1)}, u32[]{:S(2)}, u32[]{:S(2)}) %collective-permute-start.7) | collective-permute-done | bytes 1048608 | tf_op jit(solution)/shard_map/ppermute | solution.py:564
  138.5 2.5 %add_convert_fusion = bf16[128,4096]{1,0:T(8,128)(2,1)} fusion(bf16[128,4096]{1,0:T(8,128)(2,1)} %collective-permute-done.7, f32[128,4096]{1,0:T(8,128)S(1)} %fusion.3, bf16[128,4096]{1,0:T(8,128)(2,1)S(1)} %collective-permute-done.6), kind=kLoop, calls=%fused_computation.2 | loop fusion | flops 2621440 | bytes 5242880 | tf_op jit(solution)/shard_map/convert_element_type | solution.py:569
  (46 shorter events, 14.1 us)
Async XLA Ops:
  0.6 2.9 %collective-permute-start = (bf16[128,4096]{1,0:T(8,128)(2,1)}, bf16[128,4096]{1,0:T(8,128)(2,1)S(1)}, u32[]{:S(2)}, u32[]{:S(2)}) collective-permute-start(bf16[128,4096]{1,0:T(8,128)(2,1)} %mine_ref.1), channel_id=1, source_target_pairs={{0,1},{1,0},{2,3},{3,2},{4,5},{5,4},{6,7},{7,6},{8,9},{9,8},{10,11... | collective-permute-start | bytes 3145736 | tf_op jit(solution)/shard_map/ppermute | solution.py:455
  0.7 26.2 %collective-permute-start.1 = (bf16[128,4096]{1,0:T(8,128)(2,1)}, bf16[128,4096]{1,0:T(8,128)(2,1)S(1)}, u32[]{:S(2)}, u32[]{:S(2)}) collective-permute-start(bf16[128,4096]{1,0:T(8,128)(2,1)} %mine_ref.1), channel_id=1, source_target_pairs={{0,2},{1,3},{2,0},{3,1},{4,6},{5,7},{6,4},{7,5},{8,10},{9,11},{10,... | collective-permute-start | bytes 3145736 | tf_op jit(solution)/shard_map/ppermute | solution.py:454
  3.6 2.2 %copy-start = (bf16[4096,512]{1,0:T(8,128)(2,1)S(1)}, bf16[4096,512]{1,0:T(8,128)(2,1)}, u32[]{:S(2)}) copy-start(bf16[4096,512]{1,0:T(8,128)(2,1)} %wq_ref.3) | copy-start | bytes 12582916
  5.8 2.2 %copy-start.2 = (bf16[4096,512]{1,0:T(8,128)(2,1)S(1)}, bf16[4096,512]{1,0:T(8,128)(2,1)}, u32[]{:S(2)}) copy-start(bf16[4096,512]{1,0:T(8,128)(2,1)} %wk_ref.3) | copy-start | bytes 12582916
  7.9 1.2 copy-start.4
  20.7 25.7 %all-to-all-start = ((bf16[8,96,512]{2,1,0:T(8,128)(2,1)}), bf16[8,96,512]{2,1,0:T(8,128)(2,1)S(1)}, u32[]{:S(2)}, u32[]{:S(2)}) async-start(bf16[8,96,512]{2,1,0:T(8,128)(2,1)} %bitcast.5), calls=%async_computation | async-start | bytes 1572864 | tf_op jit(solution)/shard_map/all_to_all | solution.py:484
  26.9 2.7 %collective-permute-start.2 = (bf16[128,4096]{1,0:T(8,128)(2,1)S(1)}, bf16[128,4096]{1,0:T(8,128)(2,1)S(1)}, u32[]{:S(2)}, u32[]{:S(2)}) collective-permute-start(bf16[128,4096]{1,0:T(8,128)(2,1)S(1)} %collective-permute-done.1.mine_ref), channel_id=1, source_target_pairs={{0,1},{1,0},{2,3},{3,2},{4,5},{5,4},{6,7},{7,6},{8,9},{9,8},{10,11... | collective-permute-start | bytes 3145736 | tf_op jit(solution)/shard_map/ppermute | solution.py:490
  29.6 2.2 %copy-start.1 = (bf16[4096,512]{1,0:T(8,128)(2,1)S(1)}, bf16[4096,512]{1,0:T(8,128)(2,1)}, u32[]{:S(2)}) copy-start(bf16[4096,512]{1,0:T(8,128)(2,1)} %wq_ref.3) | copy-start | bytes 12582916
  31.7 2.2 %copy-start.3 = (bf16[4096,512]{1,0:T(8,128)(2,1)S(1)}, bf16[4096,512]{1,0:T(8,128)(2,1)}, u32[]{:S(2)}) copy-start(bf16[4096,512]{1,0:T(8,128)(2,1)} %wk_ref.3) | copy-start | bytes 12582916
  45.5 0.9 copy-start.5
  46.4 23.2 %all-to-all-start.1 = ((bf16[8,96,512]{2,1,0:T(8,128)(2,1)}), bf16[8,96,512]{2,1,0:T(8,128)(2,1)S(1)}, u32[]{:S(2)}, u32[]{:S(2)}) async-start(bf16[8,96,512]{2,1,0:T(8,128)(2,1)} %bitcast.7), calls=%async_computation.1 | async-start | bytes 1572864 | tf_op jit(solution)/shard_map/all_to_all | solution.py:484
  53.4 30.1 %collective-permute-start.3 = (bf16[2,64,512]{2,1,0:T(8,128)(2,1)S(1)}, bf16[2,64,512]{2,1,0:T(8,128)(2,1)S(1)}, u32[]{:S(2)}, u32[]{:S(2)}) collective-permute-start(bf16[2,64,512]{2,1,0:T(8,128)(2,1)S(1)} %get-tuple-element.33), channel_id=1, source_target_pairs={{0,4},{4,8},{8,12},{12,16},{16,20},{20,24},{24,28},{1,5},{5,9},{9,... | collective-permute-start | bytes 393224 | tf_op jit(solution)/shard_map/ppermute | solution.py:21
  56.8 26.8 %collective-permute-start.4 = (bf16[2,64,512]{2,1,0:T(8,128)(2,1)S(1)}, bf16[2,64,512]{2,1,0:T(8,128)(2,1)S(1)}, u32[]{:S(2)}, u32[]{:S(2)}) collective-permute-start(bf16[2,64,512]{2,1,0:T(8,128)(2,1)S(1)} %get-tuple-element.32), channel_id=1, source_target_pairs={{4,0},{8,4},{12,8},{16,12},{20,16},{24,20},{28,24},{5,1},{9,5},{13... | collective-permute-start | bytes 393224 | tf_op jit(solution)/shard_map/ppermute | solution.py:21
  75.8 15.0 %all-to-all-start.3 = ((bf16[8,32,640]{2,1,0:T(8,128)(2,1)}), bf16[8,32,640]{2,1,0:T(8,128)(2,1)S(1)}, u32[]{:S(2)}, u32[]{:S(2)}) async-start(bf16[8,32,640]{2,1,0:T(8,128)(2,1)} %far_wide.1), calls=%async_computation.3 | async-start | bytes 655360 | tf_op jit(solution)/shard_map/all_to_all | solution.py:484
  83.5 1.1 copy-start.6
  89.3 0.8 copy-start.7
  90.8 1.0 copy-start.8
  91.8 0.9 copy-start.10
  92.8 2.2 %copy-start.11 = (bf16[512,4096]{1,0:T(8,128)(2,1)S(1)}, bf16[512,4096]{1,0:T(8,128)(2,1)}, u32[]{:S(2)}) copy-start(bf16[512,4096]{1,0:T(8,128)(2,1)} %param.9) | copy-start | bytes 12582916
  96.7 12.2 %collective-permute-start.5 = (bf16[128,4096]{1,0:T(8,128)(2,1)}, bf16[128,4096]{1,0:T(8,128)(2,1)}, u32[]{:S(2)}, u32[]{:S(2)}) collective-permute-start(bf16[128,4096]{1,0:T(8,128)(2,1)} %convolution_convert_fusion.1), channel_id=1, source_target_pairs={{0,1},{1,0},{2,3},{3,2},{4,5},{5,4},{6,7},{7,6},{8,9},{9,8},{10,11... | collective-permute-start | bytes 3145736 | tf_op jit(solution)/shard_map/ppermute | solution.py:562
  102.9 14.7 %all-to-all-start.2 = ((bf16[8,32,640]{2,1,0:T(8,128)(2,1)}), bf16[8,32,640]{2,1,0:T(8,128)(2,1)S(1)}, u32[]{:S(2)}, u32[]{:S(2)}) async-start(bf16[8,32,640]{2,1,0:T(8,128)(2,1)} %near_wide.1), calls=%async_computation.2 | async-start | bytes 655360 | tf_op jit(solution)/shard_map/all_to_all | solution.py:484
  113.2 25.3 %collective-permute-start.7 = (bf16[128,4096]{1,0:T(8,128)(2,1)}, bf16[128,4096]{1,0:T(8,128)(2,1)}, u32[]{:S(2)}, u32[]{:S(2)}) collective-permute-start(bf16[128,4096]{1,0:T(8,128)(2,1)} %add_convert_fusion.1), channel_id=1, source_target_pairs={{0,2},{1,3},{2,0},{3,1},{4,6},{5,7},{6,4},{7,5},{8,10},{9,11},{10,... | collective-permute-start | bytes 3145736 | tf_op jit(solution)/shard_map/ppermute | solution.py:564
  117.6 2.2 %copy-start.12 = (bf16[512,4096]{1,0:T(8,128)(2,1)S(1)}, bf16[512,4096]{1,0:T(8,128)(2,1)}, u32[]{:S(2)}) copy-start(bf16[512,4096]{1,0:T(8,128)(2,1)} %param.9) | copy-start | bytes 12582916
  120.5 18.0 %collective-permute-start.6 = (bf16[128,4096]{1,0:T(8,128)(2,1)S(1)}, bf16[128,4096]{1,0:T(8,128)(2,1)S(1)}, u32[]{:S(2)}, u32[]{:S(2)}) collective-permute-start(bf16[128,4096]{1,0:T(8,128)(2,1)S(1)} %convolution_convert_fusion), channel_id=1, source_target_pairs={{0,1},{1,0},{2,3},{3,2},{4,5},{5,4},{6,7},{7,6},{8,9},{9,8},{10,11... | collective-permute-start | bytes 3145736 | tf_op jit(solution)/shard_map/ppermute | solution.py:567
  (1 other events, 0.7 us)

commit v2 on v1

--- a/solution.py
+++ b/solution.py
@@ -216,13 +216,6 @@
     return block * cosine + other * sine
 
 
-def fill_pair(place, mine_ref, peer_ref, xs):
-    rows = mine_ref.shape[0]
-    core = place[1]
-    xs[pl.ds(pl.multiple_of(core * rows, rows), rows), :] = mine_ref[...]
-    xs[pl.ds(pl.multiple_of((1 - core) * rows, rows), rows), :] = peer_ref[...]
-
-
 def low_part(x, size):
     return jnp.bitwise_and(x, size - 1)
 
@@ -231,33 +224,30 @@
     return jnp.right_shift(x, size.bit_length() - 1)
 
 
-def project_kernel(
-    place, mine_ref, peer_ref, wq_ref, wk_ref, wv_ref, cos_ref, sin_ref, qkv_ref, send_ref, xs,
-):
+def finish_kernel(place, *refs):
+    mine_refs, peer_refs = refs[:3], refs[3:6]
+    cos_ref, sin_ref, qkv_ref, send_ref = refs[6:]
     rows = qkv_ref.shape[1]
-    cols = qkv_ref.shape[2]
+    block = rows // 2
     classes, _, per_class, _ = send_ref.shape
-    fill_pair(place, mine_ref, peer_ref, xs)
+    for refs_of, core in ((mine_refs, place[1]), (peer_refs, 1 - place[1])):
+        at = pl.ds(pl.multiple_of(core * block, block), block)
+        for n in range(3):
+            part = refs_of[n][...]
+            if n < 2:
+                part = turned(part, cos_ref[at, :], sin_ref[at, :])
+            if n == 0:
+                part = part * HEAD_DIM ** (-0.5)
+            qkv_ref[n, at, :] = part.astype(jnp.bfloat16)
     target = lax.broadcasted_iota(jnp.int32, (rows, rows), 0)
     source = lax.broadcasted_iota(jnp.int32, (rows, rows), 1)
     wanted = low_part(target, per_class) * classes + high_part(target, per_class)
     perm = jnp.where(source == wanted, 1.0, 0.0).astype(jnp.bfloat16)
-    scale = HEAD_DIM ** (-0.5)
-    width = 256
-    for at in range(0, cols, width):
-        cut = slice(at, at + width)
-        for n, w_ref in enumerate((wq_ref, wk_ref, wv_ref)):
-            part = jnp.dot(xs[...], w_ref[:, cut], preferred_element_type=jnp.float32)
-            if n < 2:
-                part = turned(part, cos_ref[...], sin_ref[...])
-            if n == 0:
-                part = part * scale
-            part = part.astype(jnp.bfloat16)
-            qkv_ref[n, :, cut] = part
-            moved = jnp.dot(perm, part, preferred_element_type=jnp.float32)
-            moved = moved.astype(jnp.bfloat16)
-            for c in range(classes):
-                send_ref[c, n, :, cut] = moved[c * per_class : (c + 1) * per_class]
+    for n in range(3):
+        moved = jnp.dot(perm, qkv_ref[n], preferred_element_type=jnp.float32)
+        moved = moved.astype(jnp.bfloat16)
+        for c in range(classes):
+            send_ref[c, n] = moved[c * per_class : (c + 1) * per_class]
 
 
 def soft_pair(q, k, v, bias):
@@ -434,7 +424,6 @@
     return pl.CostEstimate(flops=int(flops), bytes_accessed=int(size), transcendentals=0)
 
 
-PROJECT_MIB = 40
 SCALARS = pl.BlockSpec(memory_space=pltpu.SMEM)
 
 
@@ -463,20 +452,23 @@
     bf16 = jnp.bfloat16
     whole = pl.BlockSpec(memory_space=pltpu.VMEM)
 
-    def project(mine, peer, tables, name):
+    def project(x):
+        weights = (w_query, w_key, w_value)
+        return [jnp.dot(x, w, preferred_element_type=jnp.float32) for w in weights]
+
+    def finish(mine, peer, tables, name):
         return pl.pallas_call(
-            project_kernel,
-            in_specs=[SCALARS] + [whole] * 7,
+            finish_kernel,
+            in_specs=[SCALARS] + [whole] * 8,
             out_specs=[whole, whole],
             out_shape=[
                 jax.ShapeDtypeStruct((3, half, cols), bf16),
                 jax.ShapeDtypeStruct((sp_size, 3, share, cols), bf16),
             ],
-            scratch_shapes=[pltpu.VMEM((half, depth), bf16)],
-            compiler_params=pltpu.CompilerParams(vmem_limit_bytes=PROJECT_MIB * 2**20),
-            cost_estimate=cost(2 * half * depth * 3 * cols, 3 * depth * cols * 2),
+            compiler_params=pltpu.CompilerParams(vmem_limit_bytes=16 * 2**20),
+            cost_estimate=cost(2e9, 3 * half * cols * 10),
             name=name,
-        )(place, mine, peer, w_query, w_key, w_value, *tables)
+        )(place, *mine, *peer, *tables)
 
     def exchange(block):
         shape = block.shape
@@ -484,11 +476,11 @@
         flat = lax.all_to_all(flat, "sp", split_axis=0, concat_axis=0, tiled=True)
         return flat.reshape(shape)
 
-    near, near_send = project(tokens_in, near_peer, near_tables, "near_project")
+    near, near_send = finish(project(tokens_in), project(near_peer), near_tables, "near_finish")
     near_all = exchange(near_send)
     near, far_mine = lax.optimization_barrier((near, far_mine))
     far_peer = lax.ppermute(far_mine, "tp", beside)
-    far, far_send = project(far_mine, far_peer, far_tables, "far_project")
+    far, far_send = finish(project(far_mine), project(far_peer), far_tables, "far_finish")
     far_all = exchange(far_send)
     low = jnp.where(y_place == 0, near[1:, :SIDE_SPAN], far[1:, :SIDE_SPAN])
     top = jnp.where(y_place == 0, far[1:, half - SIDE_SPAN :], near[1:, half - SIDE_SPAN :])
@@ -549,11 +541,12 @@
             name=name,
         )(place, o_near, l_near, returned)
 
+    far_all, near_all, o_near, l_near = lax.optimization_barrier((far_all, near_all, o_near, l_near))
     far_wide = wide(1 - y_place, far_all, near_all, "far_wide")
     far_back = exchange(far_wide)
     near_first, near_second, _ = lax.optimization_barrier((near_all, far_all, far_wide))
     near_wide = wide(y_place, near_first, near_second, "near_wide")
-    near_back = exchange(near_wide)
+    far_back, near_wide = lax.optimization_barrier((far_back, near_wide))
     far_att, far_lw = merge(1, far_back, "far_merge")
 
     def product(block):
@@ -561,8 +554,9 @@
 
     first = lax.ppermute(product(far_att[:own_rows]).astype(bf16), "tp", beside)
     second = (product(far_att[own_rows:]) + first.astype(jnp.float32)).astype(bf16)
+    near_wide, second = lax.optimization_barrier((near_wide, second))
     crossed = lax.ppermute(second, "tp", cross)
-    near_back, second = lax.optimization_barrier((near_back, second))
+    near_back = exchange(near_wide)
     near_att, near_lw = merge(0, near_back, "near_merge")
     third = lax.ppermute(product(near_att[:own_rows]).astype(bf16), "tp", beside)
     total = product(near_att[own_rows:]) + third.astype(jnp.float32)

time: 143 us -> 143 us (level)
  waiting for transfers between devices: 34.4 us -> 54.8 us
  Pallas kernels: 43.8 us -> 25.8 us
  local copies, waits for them, and re-layouts: 16.1 us -> 3.09 us
  matrix products: 7.52 us -> 19.9 us
  starting transfers between devices: 33.1 us -> 31.4 us
    pallas_call x2, Pallas kernels: 23 us -> 5.06 us  [finish(): pl.pallas_call(finish_kernel, in_specs=[SCALARS] + [whole] * 8, out_specs...]
    dot_general x0 -> x12, matrix products: none -> 16.9 us  [project(): return [jnp.dot(x, w, preferred_element_type=jnp.float32) for w in weights]]
    ppermute x2, waiting for transfers between devices: 0.01 us -> 14 us  [shifted(): return lax.ppermute(block, axis, route)]
    ppermute x1, waiting for transfers between devices: 0.01 us -> 13.1 us  [fast_device(): far_mine = lax.ppermute(tokens_in, 'tp', cross)]
    unnamed x26, local copies, waits for them, and re-layouts: 16.1 us -> 3.09 us
    dot_general x4, matrix products: 7.52 us -> 2.98 us  [product(): return jnp.dot(block, w_out, preferred_element_type=jnp.float32)]
    ppermute x1, waiting for transfers between devices: 16.5 us -> 12 us  [fast_device(): crossed = lax.ppermute(second, 'tp', cross)]
    ppermute x1, waiting for transfers between devices: 2.65 us -> 0.01 us  [fast_device(): far_peer = lax.ppermute(far_mine, 'tp', beside)]
  transfers between devices with their start and end apart: 12 -> 12, of which waited for: 5 -> 7; matrix products, arithmetic and copies ran while one was open for 6% -> 15% of each run, Pallas kernels for 30% -> 13%
where the time goes in v2:
time: 143 us; the launch traced here: 141 us
  waiting for transfers between devices  54.8 us (38%)
  starting transfers between devices  31.4 us (22%)
  Pallas kernels  25.8 us (18%)
  matrix products  19.9 us (14%)
  other arithmetic  5.07 us (4%)
  local copies, waits for them, and re-layouts  3.09 us (2%)
    all_to_all x4, starting transfers between devices, exchange(): flat = lax.all_to_all(flat, 'sp', split_axis=0, concat_axis=0, tiled=True)  23.3 us
    dot_general x12, matrix products, project(): return [jnp.dot(x, w, preferred_element_type=jnp.float32) for w in weights]  16.9 us
    ppermute x2, waiting for transfers between devices, shifted(): return lax.ppermute(block, axis, route)  14 us
    ppermute x1, waiting for transfers between devices, fast_device(): far_mine = lax.ppermute(tokens_in, 'tp', cross)  13.1 us
    all_to_all x4, waiting for transfers between devices, exchange(): flat = lax.all_to_all(flat, 'sp', split_axis=0, concat_axis=0, tiled=True)  13 us
    pallas_call x2, Pallas kernels, wide(): pl.pallas_call(lambda *refs: wide_kernel(MIDDLE_DILATION // sp_size, WIDE...  12.4 us
    ppermute x1, waiting for transfers between devices, fast_device(): crossed = lax.ppermute(second, 'tp', cross)  12 us
    ppermute x2, starting transfers between devices, shifted(): return lax.ppermute(block, axis, route)  6.91 us
  transfers between devices with their start and end apart: 12, of which 7 were waited for; matrix products, arithmetic and copies ran while one was open for 15% of the time, Pallas kernels for 13%

profile of v2, /device:TPU:14, one launch (start us, length us, event | category | flops | bytes accessed | tf_op | source)
XLA Modules:
  0.0 141.0 jit_solution(2505495624489154365)
XLA Ops:
  2.4 3.4 %fusion.14.refs_0_ = f32[128,512]{1,0:T(8,128)S(1)} fusion(bf16[128,4096]{1,0:T(8,128)(2,1)} %param.5, bf16[4096,512]{1,0:T(8,128)(2,1)} %param.6), kind=kOutput, calls=%fused_computation.32 | convolution fusion | flops 536870912 | bytes 5505024 | tf_op jit(solution)/shard_map/dot_general | solution.py:457
  10.3 2.5 %near_finish.1 = (bf16[3,256,512]{2,1,0:T(8,128)(2,1)S(1)}, bf16[8,3,32,512]{3,2,1,0:T(8,128)(2,1)}) custom-call(s32[2]{0:T(128)S(1)} %pad_add_fusion.place.refs_0_, f32[128,512]{1,0:T(8,128)S(1)} %fusion.14.refs_0_, f32[128,512]{1,0:T(8,128)S(1)} %fusion.15.refs_1_, f32[128,512]{1,0:T(8,128)S(1)} %fusion.16.refs_2_, f32[128,512]{1,0:T(8,128)S(1)} %fusion.17.refs_3_, ...), custom_call_target="tpu_custom_call" | custom-call | flops 2000000000 | bytes 3932160 | tf_op jit(solution)/shard_map/near_finish/pallas_call | solution.py:460
  12.8 13.1 %collective-permute-done.1 = bf16[128,4096]{1,0:T(8,128)(2,1)} collective-permute-done((bf16[128,4096]{1,0:T(8,128)(2,1)}, bf16[128,4096]{1,0:T(8,128)(2,1)}, u32[]{:S(2)}, u32[]{:S(2)}) %collective-permute-start.1) | collective-permute-done | bytes 1048608 | tf_op jit(solution)/shard_map/ppermute | solution.py:443
  25.9 6.2 %all-to-all-start.1 = ((bf16[8,96,512]{2,1,0:T(8,128)(2,1)}), bf16[8,96,512]{2,1,0:T(8,128)(2,1)S(1)}, u32[]{:S(2)}, u32[]{:S(2)}) async-start(bf16[8,96,512]{2,1,0:T(8,128)(2,1)} %bitcast.4), calls=%async_computation.1 | async-start | bytes 1572864 | tf_op jit(solution)/shard_map/all_to_all | solution.py:476
  32.2 3.4 %fusion.22.refs_2_ = f32[128,512]{1,0:T(8,128)S(1)} fusion(bf16[128,4096]{1,0:T(8,128)(2,1)} %collective-permute-done.1, bf16[4096,512]{1,0:T(8,128)(2,1)} %param.8), kind=kOutput, calls=%fused_computation.40 | convolution fusion | flops 536870912 | bytes 5505024 | tf_op jit(solution)/shard_map/dot_general | solution.py:457
  35.9 2.2 %fusion.21.refs_1_ = f32[128,512]{1,0:T(8,128)S(1)} fusion(bf16[128,4096]{1,0:T(8,128)(2,1)} %collective-permute-done.1, bf16[4096,512]{1,0:T(8,128)(2,1)S(1)} %copy-done.7), kind=kOutput, calls=%fused_computation.39 | convolution fusion | flops 536870912 | bytes 5505024 | tf_op jit(solution)/shard_map/dot_general | solution.py:457
  38.1 1.9 %fusion.20.refs_0_ = f32[128,512]{1,0:T(8,128)S(1)} fusion(bf16[128,4096]{1,0:T(8,128)(2,1)} %collective-permute-done.1, bf16[4096,512]{1,0:T(8,128)(2,1)S(1)} %copy-done.9), kind=kOutput, calls=%fused_computation.38 | convolution fusion | flops 536870912 | bytes 5505024 | tf_op jit(solution)/shard_map/dot_general | solution.py:457
  42.2 2.5 %far_finish.1 = (bf16[3,256,512]{2,1,0:T(8,128)(2,1)S(1)}, bf16[8,3,32,512]{3,2,1,0:T(8,128)(2,1)}) custom-call(s32[2]{0:T(128)S(1)} %pad_add_fusion.place.refs_0_, f32[128,512]{1,0:T(8,128)S(1)} %fusion.20.refs_0_, f32[128,512]{1,0:T(8,128)S(1)} %fusion.21.refs_1_, f32[128,512]{1,0:T(8,128)S(1)} %fusion.22.refs_2_, f32[128,512]{1,0:T(8,128)S(1)} %fusion.23.refs_3_, ...), custom_call_target="tpu_custom_call" | custom-call | flops 2000000000 | bytes 3932160 | tf_op jit(solution)/shard_map/far_finish/pallas_call | solution.py:460
  44.8 3.4 %all-to-all-done.1 = bf16[8,96,512]{2,1,0:T(8,128)(2,1)S(1)} async-done(((bf16[8,96,512]{2,1,0:T(8,128)(2,1)}), bf16[8,96,512]{2,1,0:T(8,128)(2,1)S(1)}, u32[]{:S(2)}, u32[]{:S(2)}) %all-to-all-start.1) | async-done | bytes 786464 | tf_op jit(solution)/shard_map/all_to_all | solution.py:476
  48.2 6.9 %all-to-all-start = ((bf16[8,96,512]{2,1,0:T(8,128)(2,1)}), bf16[8,96,512]{2,1,0:T(8,128)(2,1)S(1)}, u32[]{:S(2)}, u32[]{:S(2)}) async-start(bf16[8,96,512]{2,1,0:T(8,128)(2,1)} %bitcast.2), calls=%async_computation | async-start | bytes 1572864 | tf_op jit(solution)/shard_map/all_to_all | solution.py:476
  55.8 2.5 %collective-permute-start.4 = (bf16[2,64,512]{2,1,0:T(8,128)(2,1)}, bf16[2,64,512]{2,1,0:T(8,128)(2,1)S(1)}, u32[]{:S(2)}, u32[]{:S(2)}) collective-permute-start(bf16[2,64,512]{2,1,0:T(8,128)(2,1)} %get-tuple-element.46), channel_id=1, source_target_pairs={{4,0},{8,4},{12,8},{16,12},{20,16},{24,20},{28,24},{5,1},{9,5},{13... | collective-permute-start | bytes 393224 | tf_op jit(solution)/shard_map/ppermute | solution.py:21
  58.2 4.5 %collective-permute-start.3 = (bf16[2,64,512]{2,1,0:T(8,128)(2,1)S(1)}, bf16[2,64,512]{2,1,0:T(8,128)(2,1)S(1)}, u32[]{:S(2)}, u32[]{:S(2)}) collective-permute-start(bf16[2,64,512]{2,1,0:T(8,128)(2,1)S(1)} %get-tuple-element.47), channel_id=1, source_target_pairs={{0,4},{4,8},{8,12},{12,16},{16,20},{20,24},{24,28},{1,5},{5,9},{9,... | collective-permute-start | bytes 393224 | tf_op jit(solution)/shard_map/ppermute | solution.py:21
  62.8 14.0 %collective-permute-done.4.after_ref = bf16[2,64,512]{2,1,0:T(8,128)(2,1)S(1)} collective-permute-done((bf16[2,64,512]{2,1,0:T(8,128)(2,1)}, bf16[2,64,512]{2,1,0:T(8,128)(2,1)S(1)}, u32[]{:S(2)}, u32[]{:S(2)}) %collective-permute-start.4) | collective-permute-done | bytes 131104 | tf_op jit(solution)/shard_map/ppermute | solution.py:21
  76.8 4.6 %local_attend.1 = (bf16[2,256,512]{2,1,0:T(8,128)(2,1)S(1)}, f32[2,256,128]{2,1,0:T(8,128)S(1)}) custom-call(s32[3]{0:T(128)S(1)} %add_convert_fusion.2.info, bf16[3,256,512]{2,1,0:T(8,128)(2,1)S(1)} %get-tuple-element.28.near_ref, bf16[3,256,512]{2,1,0:T(8,128)(2,1)S(1)} %get-tuple-element.29.far_ref, ...), custom_call_target="tpu_custom_call" | custom-call | flops 6000000000 | bytes 4000000 | tf_op jit(solution)/shard_map/local_attend/pallas_call | solution.py:493
  82.9 6.2 %far_wide.1 = bf16[8,32,640]{2,1,0:T(8,128)(2,1)} custom-call(s32[1]{0:T(128)} %bitcast.9.refs_0_, bf16[8,3,32,512]{3,2,1,0:T(8,128)(2,1)S(1)} %bitcast.40, bf16[8,3,32,512]{3,2,1,0:T(8,128)(2,1)S(1)} %bitcast.38), custom_call_target="tpu_custom_call" | custom-call | flops 6000000000 | bytes 4000000 | tf_op jit(solution)/shard_map/far_wide/pallas_call | solution.py:514
  89.1 4.2 %all-to-all-start.2 = ((bf16[8,32,640]{2,1,0:T(8,128)(2,1)}), bf16[8,32,640]{2,1,0:T(8,128)(2,1)S(1)}, u32[]{:S(2)}, u32[]{:S(2)}) async-start(bf16[8,32,640]{2,1,0:T(8,128)(2,1)} %far_wide.1), calls=%async_computation.2 | async-start | bytes 655360 | tf_op jit(solution)/shard_map/all_to_all | solution.py:476
  93.3 6.2 %near_wide.1 = bf16[8,32,640]{2,1,0:T(8,128)(2,1)} custom-call(s32[1]{0:T(128)} %bitcast.refs_0_, bf16[8,3,32,512]{3,2,1,0:T(8,128)(2,1)S(1)} %bitcast.39, bf16[8,3,32,512]{3,2,1,0:T(8,128)(2,1)S(1)} %bitcast.41), custom_call_target="tpu_custom_call" | custom-call | flops 6000000000 | bytes 4000000 | tf_op jit(solution)/shard_map/near_wide/pallas_call | solution.py:514
  101.3 1.9 %far_merge.1 = (bf16[256,512]{1,0:T(8,128)(2,1)S(1)}, f32[8,256]{1,0:T(8,128)S(1)}) custom-call(s32[2]{0:T(128)S(1)} %pad_add_fusion.place.refs_0_, bf16[2,256,512]{2,1,0:T(8,128)(2,1)S(1)} %copy-done.1, f32[2,256,128]{2,1,0:T(8,128)S(1)} %copy-done.3, bf16[8,32,640]{2,1,0:T(8,128)(2,1)S(1)} %all-to-all-done.2.refs_3_), custom_call_target="tpu_custom_call" | custom-call | flops 2000000000 | bytes 4000000 | tf_op jit(solution)/shard_map/far_merge/pallas_call | solution.py:530
  104.3 2.6 %collective-permute-done.5 = bf16[128,4096]{1,0:T(8,128)(2,1)S(1)} collective-permute-done((bf16[128,4096]{1,0:T(8,128)(2,1)S(1)}, bf16[128,4096]{1,0:T(8,128)(2,1)S(1)}, u32[]{:S(2)}, u32[]{:S(2)}) %collective-permute-start.5) | collective-permute-done | bytes 1048608 | tf_op jit(solution)/shard_map/ppermute | solution.py:555
  107.7 6.0 %all-to-all-start.3 = ((bf16[8,32,640]{2,1,0:T(8,128)(2,1)}), bf16[8,32,640]{2,1,0:T(8,128)(2,1)S(1)}, u32[]{:S(2)}, u32[]{:S(2)}) async-start(bf16[8,32,640]{2,1,0:T(8,128)(2,1)} %near_wide.1), calls=%async_computation.3 | async-start | bytes 655360 | tf_op jit(solution)/shard_map/all_to_all | solution.py:476
  114.2 7.8 %all-to-all-done.3.refs_3_ = bf16[8,32,640]{2,1,0:T(8,128)(2,1)S(1)} async-done(((bf16[8,32,640]{2,1,0:T(8,128)(2,1)}), bf16[8,32,640]{2,1,0:T(8,128)(2,1)S(1)}, u32[]{:S(2)}, u32[]{:S(2)}) %all-to-all-start.3) | async-done | bytes 327712 | tf_op jit(solution)/shard_map/all_to_all | solution.py:476
  122.0 1.9 %near_merge.1 = (bf16[256,512]{1,0:T(8,128)(2,1)S(1)}, f32[8,256]{1,0:T(8,128)S(1)}) custom-call(s32[2]{0:T(128)S(1)} %pad_add_fusion.place.refs_0_, bf16[2,256,512]{2,1,0:T(8,128)(2,1)S(1)} %copy-done.1, f32[2,256,128]{2,1,0:T(8,128)S(1)} %copy-done.3, bf16[8,32,640]{2,1,0:T(8,128)(2,1)S(1)} %all-to-all-done.3.refs_3_), custom_call_target="tpu_custom_call" | custom-call | flops 2000000000 | bytes 4000000 | tf_op jit(solution)/shard_map/near_merge/pallas_call | solution.py:530
  126.4 12.0 %collective-permute-done.7 = bf16[128,4096]{1,0:T(8,128)(2,1)} collective-permute-done((bf16[128,4096]{1,0:T(8,128)(2,1)S(1)}, bf16[128,4096]{1,0:T(8,128)(2,1)}, u32[]{:S(2)}, u32[]{:S(2)}) %collective-permute-start.7) | collective-permute-done | bytes 1048608 | tf_op jit(solution)/shard_map/ppermute | solution.py:558
  138.4 2.6 %add_convert_fusion = bf16[128,4096]{1,0:T(8,128)(2,1)} fusion(bf16[128,4096]{1,0:T(8,128)(2,1)} %collective-permute-done.7, f32[128,4096]{1,0:T(8,128)S(1)} %fusion.3, bf16[128,4096]{1,0:T(8,128)(2,1)S(1)} %collective-permute-done.6), kind=kLoop, calls=%fused_computation.2 | loop fusion | flops 2621440 | bytes 5242880 | tf_op jit(solution)/shard_map/convert_element_type | solution.py:563
  (58 shorter events, 17.6 us)
Async XLA Ops:
  0.6 5.1 %copy-start.12 = (bf16[128,4096]{1,0:T(8,128)(2,1)S(1)}, bf16[128,4096]{1,0:T(8,128)(2,1)}, u32[]{:S(2)}) copy-start(bf16[128,4096]{1,0:T(8,128)(2,1)} %param.5) | copy-start | bytes 3145732
  0.6 25.3 %collective-permute-start.1 = (bf16[128,4096]{1,0:T(8,128)(2,1)}, bf16[128,4096]{1,0:T(8,128)(2,1)}, u32[]{:S(2)}, u32[]{:S(2)}) collective-permute-start(bf16[128,4096]{1,0:T(8,128)(2,1)} %param.5), channel_id=1, source_target_pairs={{0,2},{1,3},{2,0},{3,1},{4,6},{5,7},{6,4},{7,5},{8,10},{9,11},{10,... | collective-permute-start | bytes 3145736 | tf_op jit(solution)/shard_map/ppermute | solution.py:443
  1.2 6.1 %collective-permute-start = (bf16[128,4096]{1,0:T(8,128)(2,1)}, bf16[128,4096]{1,0:T(8,128)(2,1)S(1)}, u32[]{:S(2)}, u32[]{:S(2)}) collective-permute-start(bf16[128,4096]{1,0:T(8,128)(2,1)} %param.5), channel_id=1, source_target_pairs={{0,1},{1,0},{2,3},{3,2},{4,5},{5,4},{6,7},{7,6},{8,9},{9,8},{10,11... | collective-permute-start | bytes 3145736 | tf_op jit(solution)/shard_map/ppermute | solution.py:444
  1.3 4.5 %copy-start.6 = (bf16[4096,512]{1,0:T(8,128)(2,1)S(1)}, bf16[4096,512]{1,0:T(8,128)(2,1)}, u32[]{:S(2)}) copy-start(bf16[4096,512]{1,0:T(8,128)(2,1)} %param.7) | copy-start | bytes 12582916
  2.3 4.2 %copy-start.4 = (bf16[4096,512]{1,0:T(8,128)(2,1)S(1)}, bf16[4096,512]{1,0:T(8,128)(2,1)}, u32[]{:S(2)}) copy-start(bf16[4096,512]{1,0:T(8,128)(2,1)} %param.8) | copy-start | bytes 12582916
  7.3 2.2 %copy-start.8 = (bf16[4096,512]{1,0:T(8,128)(2,1)S(1)}, bf16[4096,512]{1,0:T(8,128)(2,1)}, u32[]{:S(2)}) copy-start(bf16[4096,512]{1,0:T(8,128)(2,1)} %param.6) | copy-start | bytes 12582916
  25.9 22.2 %all-to-all-start.1 = ((bf16[8,96,512]{2,1,0:T(8,128)(2,1)}), bf16[8,96,512]{2,1,0:T(8,128)(2,1)S(1)}, u32[]{:S(2)}, u32[]{:S(2)}) async-start(bf16[8,96,512]{2,1,0:T(8,128)(2,1)} %bitcast.4), calls=%async_computation.1 | async-start | bytes 1572864 | tf_op jit(solution)/shard_map/all_to_all | solution.py:476
  32.1 3.7 %copy-start.7 = (bf16[4096,512]{1,0:T(8,128)(2,1)S(1)}, bf16[4096,512]{1,0:T(8,128)(2,1)}, u32[]{:S(2)}) copy-start(bf16[4096,512]{1,0:T(8,128)(2,1)} %param.7) | copy-start | bytes 12582916
  32.1 6.0 %copy-start.9 = (bf16[4096,512]{1,0:T(8,128)(2,1)S(1)}, bf16[4096,512]{1,0:T(8,128)(2,1)}, u32[]{:S(2)}) copy-start(bf16[4096,512]{1,0:T(8,128)(2,1)} %param.6) | copy-start | bytes 12582916
  32.1 7.9 %collective-permute-start.2 = (bf16[128,4096]{1,0:T(8,128)(2,1)}, bf16[128,4096]{1,0:T(8,128)(2,1)S(1)}, u32[]{:S(2)}, u32[]{:S(2)}) collective-permute-start(bf16[128,4096]{1,0:T(8,128)(2,1)} %collective-permute-done.1), channel_id=1, source_target_pairs={{0,1},{1,0},{2,3},{3,2},{4,5},{5,4},{6,7},{7,6},{8,9},{9,8},{10,11... | collective-permute-start | bytes 3145736 | tf_op jit(solution)/shard_map/ppermute | solution.py:482
  35.9 4.2 %copy-start.5 = (bf16[4096,512]{1,0:T(8,128)(2,1)S(1)}, bf16[4096,512]{1,0:T(8,128)(2,1)}, u32[]{:S(2)}) copy-start(bf16[4096,512]{1,0:T(8,128)(2,1)} %param.8) | copy-start | bytes 12582916
  48.2 34.7 %all-to-all-start = ((bf16[8,96,512]{2,1,0:T(8,128)(2,1)}), bf16[8,96,512]{2,1,0:T(8,128)(2,1)S(1)}, u32[]{:S(2)}, u32[]{:S(2)}) async-start(bf16[8,96,512]{2,1,0:T(8,128)(2,1)} %bitcast.2), calls=%async_computation | async-start | bytes 1572864 | tf_op jit(solution)/shard_map/all_to_all | solution.py:476
  55.8 21.0 %collective-permute-start.4 = (bf16[2,64,512]{2,1,0:T(8,128)(2,1)}, bf16[2,64,512]{2,1,0:T(8,128)(2,1)S(1)}, u32[]{:S(2)}, u32[]{:S(2)}) collective-permute-start(bf16[2,64,512]{2,1,0:T(8,128)(2,1)} %get-tuple-element.46), channel_id=1, source_target_pairs={{4,0},{8,4},{12,8},{16,12},{20,16},{24,20},{28,24},{5,1},{9,5},{13... | collective-permute-start | bytes 393224 | tf_op jit(solution)/shard_map/ppermute | solution.py:21
  58.2 18.6 %collective-permute-start.3 = (bf16[2,64,512]{2,1,0:T(8,128)(2,1)S(1)}, bf16[2,64,512]{2,1,0:T(8,128)(2,1)S(1)}, u32[]{:S(2)}, u32[]{:S(2)}) collective-permute-start(bf16[2,64,512]{2,1,0:T(8,128)(2,1)S(1)} %get-tuple-element.47), channel_id=1, source_target_pairs={{0,4},{4,8},{8,12},{12,16},{16,20},{20,24},{24,28},{1,5},{5,9},{9,... | collective-permute-start | bytes 393224 | tf_op jit(solution)/shard_map/ppermute | solution.py:21
  81.4 0.8 copy-start
  89.1 12.2 %all-to-all-start.2 = ((bf16[8,32,640]{2,1,0:T(8,128)(2,1)}), bf16[8,32,640]{2,1,0:T(8,128)(2,1)S(1)}, u32[]{:S(2)}, u32[]{:S(2)}) async-start(bf16[8,32,640]{2,1,0:T(8,128)(2,1)} %far_wide.1), calls=%async_computation.2 | async-start | bytes 655360 | tf_op jit(solution)/shard_map/all_to_all | solution.py:476
  93.3 8.0 %copy-start.1 = (bf16[2,256,512]{2,1,0:T(8,128)(2,1)S(1)}, bf16[2,256,512]{2,1,0:T(8,128)(2,1)}, u32[]{:S(2)}) copy-start(bf16[2,256,512]{2,1,0:T(8,128)(2,1)} %copy-done) | copy-start | bytes 1572868
  93.3 8.1 %copy-start.3 = (f32[2,256,128]{2,1,0:T(8,128)S(1)}, f32[2,256,128]{2,1,0:T(8,128)}, u32[]{:S(2)}) copy-start(f32[2,256,128]{2,1,0:T(8,128)} %copy-done.2) | copy-start | bytes 786436
  101.3 2.2 %copy-start.10 = (bf16[512,4096]{1,0:T(8,128)(2,1)S(1)}, bf16[512,4096]{1,0:T(8,128)(2,1)}, u32[]{:S(2)}) copy-start(bf16[512,4096]{1,0:T(8,128)(2,1)} %param.9) | copy-start | bytes 12582916
  104.3 2.7 %collective-permute-start.5 = (bf16[128,4096]{1,0:T(8,128)(2,1)S(1)}, bf16[128,4096]{1,0:T(8,128)(2,1)S(1)}, u32[]{:S(2)}, u32[]{:S(2)}) collective-permute-start(bf16[128,4096]{1,0:T(8,128)(2,1)S(1)} %convolution_convert_fusion.1), channel_id=1, source_target_pairs={{0,1},{1,0},{2,3},{3,2},{4,5},{5,4},{6,7},{7,6},{8,9},{9,8},{10,11... | collective-permute-start | bytes 3145736 | tf_op jit(solution)/shard_map/ppermute | solution.py:555
  107.7 14.2 %all-to-all-start.3 = ((bf16[8,32,640]{2,1,0:T(8,128)(2,1)}), bf16[8,32,640]{2,1,0:T(8,128)(2,1)S(1)}, u32[]{:S(2)}, u32[]{:S(2)}) async-start(bf16[8,32,640]{2,1,0:T(8,128)(2,1)} %near_wide.1), calls=%async_computation.3 | async-start | bytes 655360 | tf_op jit(solution)/shard_map/all_to_all | solution.py:476
  113.7 24.7 %collective-permute-start.7 = (bf16[128,4096]{1,0:T(8,128)(2,1)S(1)}, bf16[128,4096]{1,0:T(8,128)(2,1)}, u32[]{:S(2)}, u32[]{:S(2)}) collective-permute-start(bf16[128,4096]{1,0:T(8,128)(2,1)S(1)} %add_convert_fusion.1), channel_id=1, source_target_pairs={{0,2},{1,3},{2,0},{3,1},{4,6},{5,7},{6,4},{7,5},{8,10},{9,11},{10,... | collective-permute-start | bytes 3145736 | tf_op jit(solution)/shard_map/ppermute | solution.py:558
  122.0 2.2 %copy-start.11 = (bf16[512,4096]{1,0:T(8,128)(2,1)S(1)}, bf16[512,4096]{1,0:T(8,128)(2,1)}, u32[]{:S(2)}) copy-start(bf16[512,4096]{1,0:T(8,128)(2,1)} %param.9) | copy-start | bytes 12582916
  124.9 13.5 %collective-permute-start.6 = (bf16[128,4096]{1,0:T(8,128)(2,1)S(1)}, bf16[128,4096]{1,0:T(8,128)(2,1)S(1)}, u32[]{:S(2)}, u32[]{:S(2)}) collective-permute-start(bf16[128,4096]{1,0:T(8,128)(2,1)S(1)} %convolution_convert_fusion), channel_id=1, source_target_pairs={{0,1},{1,0},{2,3},{3,2},{4,5},{5,4},{6,7},{7,6},{8,9},{9,8},{10,11... | collective-permute-start | bytes 3145736 | tf_op jit(solution)/shard_map/ppermute | solution.py:561
  (1 other events, 0.7 us)
